TPU v7x, 256 devices: a whole 4x4x8 slice. The times are simulated.
256 devices in a mesh: sp: 32 (over z, x), tp: 8 (over y, core).
Axes of the slice: x: 4, y: 4, z: 8, core: 2. Of those that a mesh axis runs over, the one named last changes fastest.
Arguments:
- resid: bfloat16 [12288, 2048], P('sp'), may hold values from -6 to 6
- cotangent: bfloat16 [12288, 2048], P('sp'), may hold values from -0.59765625 to 0.59765625
- routes: int32 [12288, 2], P('sp'), may hold values from 0 to 31, all different within a row; in each aligned block of 384 rows (0 to 383, 384 to 767, ...) at most 48 rows name the same one
- route_weight: float32 [12288, 2], P('sp'), may hold values from 0.3 to 2.2
- w_gate: bfloat16 [32, 2048, 1024], P('sp', None, 'tp'), may hold values from -0.125 to 0.125
- w_up: bfloat16 [32, 2048, 1024], P('sp', None, 'tp'), may hold values from -0.125 to 0.125
- w_down: bfloat16 [32, 1024, 2048], P('sp', 'tp'), may hold values from -0.1875 to 0.1875
- out_proj: bfloat16 [2048, 2816], P(None, 'tp'), may hold values from -0.109375 to 0.109375
- gate_pre: bfloat16 [12288, 2816], P('sp', 'tp'), may hold values from -8 to 8
- log_decay: float32 [12288, 2816], P('sp', 'tp'), may hold values from -1 to 0
- state_before: float32 [12288, 2816], P('sp', 'tp'), may hold values from -6 to 6
- step_input: bfloat16 [12288, 2816], P('sp', 'tp'), may hold values from -6 to 6
Outputs:
- grad_gate: float32 [32, 2048, 1024], P('sp', None, 'tp')
- grad_up: float32 [32, 2048, 1024], P('sp', None, 'tp')
- grad_down: float32 [32, 1024, 2048], P('sp', 'tp')
- grad_proj: float32 [2048, 2816], P('sp', 'tp')
- grad_gate_pre: bfloat16 [12288, 2816], P('sp', 'tp')
- grad_step_input: float32 [12288, 2816], P('sp', 'tp')
- grad_log_decay: float32 [12288, 2816], P('sp', 'tp')
Inputs may be any that keep to these rules, and one draw needn't show every extreme that they name: `routes`: each row names 2 different experts. In the rows of one device no expert is named more than 48 times; some expert is named exactly 48 times in the rows of some devices.
All inputs are finite; a program needn't handle non-finite values.
Results may differ from a plain program's by a relative error of at most 0.02.
Values may be sent and summed in bfloat16 or wider, within the bound.
A program may use at most 128 MiB of HBM per device.

v0:
```python
import jax
import jax.numpy as jnp
from jax import lax
from jax.sharding import PartitionSpec as P


def side_by_side(arrays, axis, split_dim, concat_dim, along):
    widths = [a.shape[along] for a in arrays]
    both = jnp.concatenate(arrays, axis=along)
    result = lax.all_to_all(both, axis, split_axis=split_dim, concat_axis=concat_dim, tiled=True)
    return tuple(jnp.split(result, [sum(widths[:k]) for k in range(1, len(widths))], axis=along))


def side_by_side_2(arrays, axis, dim, along):
    both = jnp.concatenate(arrays, axis=along)
    result, at, finished = (lax.all_gather(both, axis, axis=dim, tiled=True), 0, [])
    for a in arrays:
        finished.append(lax.slice_in_dim(result, at, at + a.shape[along], axis=along))
        at += a.shape[along]
    return tuple(finished)


def joined_along(pieces, dim):
    lengths = list(pieces.shape[1:])
    lengths[dim] *= pieces.shape[0]
    return jnp.moveaxis(pieces, 0, dim).reshape(lengths)


def sent_to_all(shard, axis):
    copies = jnp.broadcast_to(shard, (lax.axis_size(axis), *shard.shape))
    return lax.all_to_all(copies, axis, split_axis=0, concat_axis=0, tiled=True)


def collect(shard, axis, dim):
    return joined_along(sent_to_all(shard, axis), dim)


def cut_along(shard, dim, length):
    lengths = shard.shape
    pieces = shard.reshape(*lengths[:dim], length, lengths[dim] // length, *lengths[dim + 1 :])
    return jnp.moveaxis(pieces, dim, 0)


def summed_on_arrival(shard, axis, dim):
    pieces = cut_along(shard, dim, lax.axis_size(axis))
    arrived = lax.all_to_all(pieces, axis, split_axis=0, concat_axis=0, tiled=True)
    return arrived.astype(jnp.float32).sum(axis=0)


def all_in_one(shard, axis):
    leaves = jax.tree.leaves(shard)
    sequence = sorted(range(len(leaves)), key=lambda k: -leaves[k].size)
    width = (1, *leaves[sequence[0]].shape)[-1]
    lines = [
        jnp.pad(leaves[k].reshape(-1), (0, -leaves[k].size % width)).reshape(-1, width)
        for k in sequence
    ]
    both, at, found = (sent_to_all(jnp.concatenate(lines), axis), 0, {})
    for k, line in zip(sequence, lines):
        section = both[:, at : at + len(line)].reshape(len(both), -1)
        found[k] = section[:, : leaves[k].size].reshape(-1, *leaves[k].shape)
        at += len(line)
    numbers = iter(range(len(leaves)))
    return jax.tree.map(lambda _: found[next(numbers)], shard)


def combined_pairwise(pieces, combine):
    while len(jax.tree.leaves(pieces)[0]) > 1:
        pieces = jax.vmap(combine)(
            *(jax.tree.map(lambda part: part[side::2], pieces) for side in (0, 1))
        )
    return jax.tree.map(lambda part: part[0], pieces)


def entering(shard, axis, combine, identity):
    length, mine = (lax.axis_size(axis), lax.axis_index(axis))
    passed = jnp.arange(length) > mine

    def kept(part, zero, own):
        part = jnp.where(
            passed.reshape(-1, *(1 for _ in own.shape)), part, jnp.asarray(zero, own.dtype)
        )
        return part[::-1]

    pieces = all_in_one(shard, axis)
    return combined_pairwise(jax.tree.map(kept, pieces, identity, shard), combine)


def expert_work(in_rows, cot_rows, gate_w, up_w, down_w):
    gate_act = jnp.dot(in_rows, gate_w, preferred_element_type=jnp.float32)
    up_act = jnp.dot(in_rows, up_w, preferred_element_type=jnp.float32)
    sigmoid_a = jax.nn.sigmoid(gate_act)
    hidden = (jax.nn.silu(gate_act) * up_act).astype(jnp.bfloat16)
    grad_down = lax.dot_general(
        hidden, cot_rows, (((0,), (0,)), ((), ())), preferred_element_type=jnp.float32
    )
    d_hidden = lax.dot_general(
        cot_rows, down_w, (((1,), (1,)), ((), ())), preferred_element_type=jnp.float32
    )
    slope = sigmoid_a * (1.0 + gate_act * (1.0 - sigmoid_a))
    d_gate_act = (d_hidden * up_act * slope).astype(jnp.bfloat16)
    d_up_act = (d_hidden * jax.nn.silu(gate_act)).astype(jnp.bfloat16)
    grad_gate = lax.dot_general(
        in_rows, d_gate_act, (((0,), (0,)), ((), ())), preferred_element_type=jnp.float32
    )
    grad_up = lax.dot_general(
        in_rows, d_up_act, (((0,), (0,)), ((), ())), preferred_element_type=jnp.float32
    )
    partial_value = lax.dot_general(
        d_gate_act, gate_w, (((1,), (1,)), ((), ())), preferred_element_type=jnp.float32
    )
    partial_value = partial_value + lax.dot_general(
        d_up_act, up_w, (((1,), (1,)), ((), ())), preferred_element_type=jnp.float32
    )
    rounded = lax.optimization_barrier(partial_value.astype(jnp.bfloat16))
    return (grad_gate[None], grad_up[None], grad_down[None], rounded.astype(jnp.float32))


def gather_slots(resid_part, cot_part, slot_token, slot_weight, groups, capacity):
    col_width = resid_part.shape[1]
    resid_pad = jnp.concatenate([resid_part, jnp.zeros((1, col_width), jnp.bfloat16)], axis=0)
    cot_pad = jnp.concatenate([cot_part, jnp.zeros((1, col_width), jnp.bfloat16)], axis=0)
    send_rows = resid_pad[slot_token].reshape(groups, capacity, col_width)
    send_cot = (slot_weight[:, None] * cot_pad[slot_token].astype(jnp.float32)).astype(jnp.bfloat16)
    return (send_rows, send_cot.reshape(groups, capacity, col_width))


def combine_slots(returned, cot_part, slot_ids, tok_rows, top_count):
    col_width = returned.shape[2]
    flat_back = returned.reshape(-1, col_width)
    routed = jnp.sum(
        flat_back[slot_ids].astype(jnp.float32).reshape(tok_rows, top_count, col_width), axis=1
    )
    return (cot_part.astype(jnp.float32) + routed).astype(jnp.bfloat16)


def reverse_link(former, latter):
    return (former[0] * latter[0], latter[0] * former[1] + latter[1])


def compose(earlier, later):
    return (later[0] * earlier[0], later[0] * earlier[1] + later[1])


def on_device(
    resid,
    cotangent,
    routes,
    route_weight,
    w_gate,
    w_up,
    w_down,
    out_proj,
    gate_pre,
    log_decay,
    state_before,
    step_input,
):
    tok_rows, model_width = resid.shape
    top_count = routes.shape[1]
    groups = lax.axis_size("sp")
    capacity = 2 * tok_rows * top_count // groups
    flat_ids = routes.reshape(-1)
    onehot = (flat_ids[:, None] == jnp.arange(groups, dtype=jnp.int32)[None, :]).astype(jnp.int32)
    ranking = jnp.sum((jnp.cumsum(onehot, axis=0) - onehot) * onehot, axis=1)
    slot_ids = flat_ids * capacity + ranking
    member = slot_ids[None, :] == jnp.arange(groups * capacity, dtype=jnp.int32)[:, None]
    token_ids = jnp.arange(tok_rows * top_count, dtype=jnp.int32) // top_count
    filled = jnp.any(member, axis=1)
    slot_token = jnp.where(
        filled, jnp.sum(jnp.where(member, token_ids[None, :], 0), axis=1), tok_rows
    )
    slot_weight = jnp.sum(jnp.where(member, route_weight.reshape(-1)[None, :], 0.0), axis=1)
    col_width = model_width // lax.axis_size("tp")
    col_start = lax.axis_index("tp") * col_width
    cot_part = lax.dynamic_slice_in_dim(cotangent, col_start, col_width, 1)
    resid_part = lax.dynamic_slice_in_dim(resid, col_start, col_width, 1)
    send_rows, send_cot = gather_slots(
        resid_part, cot_part, slot_token, slot_weight, groups, capacity
    )
    got_rows, got_cot = side_by_side((send_rows, send_cot), "sp", 0, 0, 1)
    full_rows, full_cot = side_by_side_2((got_rows, got_cot), "tp", 2, 0)
    grad_gate, grad_up, grad_down, partial_value = expert_work(
        full_rows.reshape(-1, model_width),
        full_cot.reshape(-1, model_width),
        w_gate[0],
        w_up[0],
        w_down[0],
    )
    summed = lax.psum_scatter(
        partial_value.reshape(groups, capacity, model_width).astype(jnp.bfloat16),
        "tp",
        scatter_dimension=2,
        tiled=True,
    )
    returned = lax.all_to_all(summed, "sp", split_axis=0, concat_axis=0, tiled=True)
    part_grad = combine_slots(returned, cot_part, slot_ids, tok_rows, top_count)
    resid_grad = collect(part_grad, "tp", 1)
    decays = jnp.exp(log_decay)
    states = decays * state_before + step_input.astype(jnp.float32)
    gelu_val, gelu_back = jax.vjp(jax.nn.gelu, gate_pre.astype(jnp.float32))
    mixed = (gelu_val * states).astype(jnp.bfloat16)
    d_mixed = jnp.dot(resid_grad, out_proj, preferred_element_type=jnp.float32)
    grad_gate_pre = gelu_back(d_mixed * states)[0].astype(jnp.bfloat16)
    grad_proj = summed_on_arrival(
        lax.dot_general(
            resid_grad, mixed, (((0,), (0,)), ((), ())), preferred_element_type=jnp.float32
        ).astype(jnp.bfloat16),
        "sp",
        0,
    )
    direct = d_mixed * gelu_val
    channels = direct.shape[1]
    following = jnp.concatenate([decays[1:], jnp.ones((1, channels), jnp.float32)], axis=0)
    products, local_vals = lax.associative_scan(
        reverse_link, (jnp.flip(following, 0), jnp.flip(direct, 0)), axis=0
    )
    products = jnp.flip(products, 0)
    local_vals = jnp.flip(local_vals, 0)
    out_scale = decays[0] * products[0]
    out_shift = decays[0] * local_vals[0]
    identity = (jnp.ones((channels,), jnp.float32), jnp.zeros((channels,), jnp.float32))
    arriving = entering((out_scale, out_shift), "sp", compose, identity)
    grad_step_input = local_vals + products * arriving[1][None, :]
    grad_log_decay = grad_step_input * decays * state_before
    return (
        grad_gate,
        grad_up,
        grad_down,
        grad_proj,
        grad_gate_pre,
        grad_step_input,
        grad_log_decay,
    )


def solution(mesh):
    return jax.shard_map(
        on_device,
        mesh=mesh,
        in_specs=(
            P("sp", None),
            P("sp", None),
            P("sp", None),
            P("sp", None),
            P("sp", None, "tp"),
            P("sp", None, "tp"),
            P("sp", "tp", None),
            P(None, "tp"),
            P("sp", "tp"),
            P("sp", "tp"),
            P("sp", "tp"),
            P("sp", "tp"),
        ),
        out_specs=(
            P("sp", None, "tp"),
            P("sp", None, "tp"),
            P("sp", "tp", None),
            P("sp", "tp"),
            P("sp", "tp"),
            P("sp", "tp"),
            P("sp", "tp"),
        ),
        check_vma=False,
    )
```

profile of v0, /device:TPU:16, one launch (start us, length us, event | category | flops | bytes accessed | tf_op | source)
XLA Modules:
  0.0 459.4 jit_solution(4751984375001868096)
XLA Ops:
  8.5 1.7 reduce-window.6
  15.2 4.8 %gather_fusion.1 = bf16[1536,256]{1,0:T(8,128)(2,1)S(1)} fusion(bf16[385,256]{1,0:T(8,128)(2,1)S(1)} %concatenate.67, s32[2048]{0:T(1024)S(1)} %pad_clamp_fusion), kind=kCustom, calls=%fused_computation.1 | custom fusion | bytes 1579008 | tf_op jit(solution)/shard_map/gather | solution.py:124
  20.0 4.8 %gather_fusion = bf16[1536,256]{1,0:T(8,128)(2,1)S(1)} fusion(bf16[385,256]{1,0:T(8,128)(2,1)S(1)} %concatenate.66, s32[2048]{0:T(1024)S(1)} %pad_clamp_fusion), kind=kCustom, calls=%fused_computation | custom fusion | bytes 1579008 | tf_op jit(solution)/shard_map/gather | solution.py:123
  25.2 51.5 %all_to_all.25 = bf16[32,96,256]{2,1,0:T(8,128)(2,1)S(1)} all-to-all(bf16[32,96,256]{2,1,0:T(8,128)(2,1)S(1)} %pad_maximum_fusion), channel_id=1, replica_groups=mesh['sp'=32,'tp'=8] {'sp'}, dimensions={0} | all-to-all | bytes 3145728 | tf_op jit(solution)/shard_map/all_to_all | solution.py:10
  78.4 69.7 %all-gather.2.cloned.1.call-done = bf16[64,48,2048]{2,1,0:T(8,128)(2,1)} async-done(((bf16[64,48,256]{2,1,0:T(8,128)(2,1)}), bf16[64,48,2048]{2,1,0:T(8,128)(2,1)}) %all-gather.2.cloned.1.call-update) | async-done | bytes 12582928 | tf_op jit(solution)/shard_map/all_gather | solution.py:16
  148.1 5.7 %fusion.55 = (bf16[32,48,2048]{2,1,0:T(8,128)(2,1)S(1)}, bf16[32,48,2048]{2,1,0:T(8,128)(2,1)S(1)}) fusion(bf16[64,48,2048]{2,1,0:T(8,128)(2,1)} %all-gather.2.cloned.1.call-done), kind=kLoop, calls=%fused_computation.156 | loop fusion | bytes 25165824 | tf_op jit(solution)/shard_map/slice | solution.py:18
  153.8 1.8 fusion.14
  155.7 1.8 fusion.17
  158.3 2.0 multiply_convert_fusion.1
  160.4 1.8 fusion.12
  162.2 4.4 add_convert_fusion
  166.7 44.4 %reduce-scatter.2.cloned.1.call-done = bf16[32,48,256]{2,1,0:T(8,128)(2,1)} async-done(((bf16[32,48,2048]{2,1,0:T(8,128)(2,1)}), bf16[32,48,256]{2,1,0:T(8,128)(2,1)}) %reduce-scatter.2.cloned.1.call-update) | async-done | bytes 786448 | tf_op jit(solution)/shard_map/reduce_scatter | solution.py:190
  211.0 10.0 %all-to-all-start.1 = ((bf16[32,48,256]{2,1,0:T(8,128)(2,1)}), bf16[32,48,256]{2,1,0:T(8,128)(2,1)S(1)}, u32[]{:S(2)}, u32[]{:S(2)}) async-start(bf16[32,48,256]{2,1,0:T(8,128)(2,1)} %reduce-scatter.2.cloned.1.call-done), calls=%async_computation.2 | async-start | bytes 1572864 | tf_op jit(solution)/shard_map/all_to_all | solution.py:196
  221.5 22.9 %all-to-all-done.1 = bf16[32,48,256]{2,1,0:T(8,128)(2,1)S(1)} async-done(((bf16[32,48,256]{2,1,0:T(8,128)(2,1)}), bf16[32,48,256]{2,1,0:T(8,128)(2,1)S(1)}, u32[]{:S(2)}, u32[]{:S(2)}) %all-to-all-start.1) | async-done | bytes 786464 | tf_op jit(solution)/shard_map/all_to_all | solution.py:196
  244.4 2.6 gather_fusion.2
  249.9 5.6 %all-to-all-start.2 = ((bf16[8,384,256]{1,2,0:T(8,128)(2,1)}), bf16[8,384,256]{1,2,0:T(8,128)(2,1)}, u32[]{:S(2)}, u32[]{:S(2)}) async-start(bf16[8,384,256]{1,2,0:T(8,128)(2,1)} %broadcast_in_dim.83), calls=%async_computation.3 | async-start | bytes 3145728 | tf_op jit(solution)/shard_map/all_to_all | solution.py:31
  256.8 1.4 slice.365
  259.6 1.4 slice.367
  262.2 1.9 copy.110
  264.1 2.1 copy.109
  266.3 2.8 slice.366
  269.0 3.7 slice.375
  272.8 3.8 slice.368
  277.1 5.6 %convolution_bitcast_fusion.2 = f32[1,2048,128]{2,1,0:T(8,128)} fusion(bf16[1536,2048]{1,0:T(8,128)(2,1)} %bitcast.73, bf16[1536,128]{1,0:T(8,128)(2,1)S(1)} %get-tuple-element.23), kind=kOutput, calls=%fused_computation.12 | convolution fusion | flops 805306368 | bytes 7733248 | tf_op jit(solution)/shard_map/dot_general | solution.py:103
  282.6 3.2 fusion.21
  286.6 2.0 slice.372
  288.6 2.0 slice.370
  294.8 1.9 fusion.58
  296.6 1.6 slice.382
  298.2 1.6 slice.387
  299.8 1.5 slice.383
  301.3 1.5 slice.385
  302.8 1.5 slice.384
  304.4 1.7 fusion.60
  306.0 1.5 slice.393
  307.5 1.5 slice.389
  309.0 1.5 slice.391
  310.5 1.5 slice.390
  312.0 1.4 fusion.61
  318.8 1.4 fusion.63
  341.1 1.5 slice.388
  342.6 1.5 slice.423
  346.0 1.5 slice.425
  353.5 1.4 slice.429
  372.0 1.7 add_multiply_fusion.2
  373.7 2.1 slice.430
  376.8 1.6 pad_maximum_fusion.3
  380.9 1.8 add_multiply_fusion
  385.2 1.7 pad.132
  387.0 2.7 pad.133
  391.1 5.6 %all-to-all-start.4 = ((f32[32,2,352]{2,1,0:T(2,128)}), f32[32,2,352]{2,1,0:T(2,128)}, u32[]{:S(2)}, u32[]{:S(2)}) async-start(f32[32,2,352]{2,1,0:T(2,128)} %broadcast_in_dim.85), calls=%async_computation.5 | async-start | bytes 196608 | tf_op jit(solution)/shard_map/all_to_all | solution.py:31
  396.7 2.8 convolution_convert_fusion
  399.5 1.6 copy.111
  401.0 5.6 %all-to-all-done.4 = f32[32,2,352]{2,1,0:T(2,128)} async-done(((f32[32,2,352]{2,1,0:T(2,128)}), f32[32,2,352]{2,1,0:T(2,128)}, u32[]{:S(2)}, u32[]{:S(2)}) %all-to-all-start.4) | async-done | bytes 90144 | tf_op jit(solution)/shard_map/all_to_all | solution.py:31
  406.6 4.8 %all-to-all-start.3 = ((bf16[32,64,352]{2,1,0:T(8,128)(2,1)}), bf16[32,64,352]{2,1,0:T(8,128)(2,1)}, u32[]{:S(2)}, u32[]{:S(2)}) async-start(bf16[32,64,352]{2,1,0:T(8,128)(2,1)} %bitcast.81), calls=%async_computation.4 | async-start | bytes 3145728 | tf_op jit(solution)/shard_map/all_to_all | solution.py:46
  411.5 5.8 %convolution_bitcast_fusion.1 = f32[1,2048,128]{2,1,0:T(8,128)} fusion(bf16[1536,2048]{1,0:T(8,128)(2,1)} %bitcast.74, bf16[1536,128]{1,0:T(8,128)(2,1)} %copy-done.24), kind=kOutput, calls=%fused_computation.11 | convolution fusion | flops 805306368 | bytes 7733248 | tf_op jit(solution)/shard_map/dot_general | solution.py:106
  417.3 2.1 convolution_bitcast_fusion
  421.3 5.4 %rev.11 = f32[384,352]{1,0:T(8,128)} reverse(f32[384,352]{1,0:T(8,128)} %add.298), dimensions={0} | reverse | bytes 1081344 | tf_op jit(solution)/shard_map/jit(_flip)/rev | solution.py:219
  426.6 5.3 %rev.12 = f32[384,352]{1,0:T(8,128)} reverse(f32[384,352]{1,0:T(8,128)} %add.306), dimensions={0} | reverse | bytes 1081344 | tf_op jit(solution)/shard_map/jit(_flip)/rev | solution.py:218
  433.9 3.1 multiply_multiply_fusion
  437.8 2.1 copy.117
  439.9 2.1 copy.118
  442.0 8.2 %all-to-all-done.3 = bf16[32,64,352]{2,1,0:T(8,128)(2,1)} async-done(((bf16[32,64,352]{2,1,0:T(8,128)(2,1)}), bf16[32,64,352]{2,1,0:T(8,128)(2,1)}, u32[]{:S(2)}, u32[]{:S(2)}) %all-to-all-start.3) | async-done | bytes 1441824 | tf_op jit(solution)/shard_map/all_to_all | solution.py:46
  450.2 2.3 convert_reduce_fusion
  (255 shorter events, 84.4 us)
Async XLA Ops:
  7.2 275.5 %copy-start = (bf16[2048,352]{0,1:T(8,128)(2,1)S(1)}, bf16[2048,352]{0,1:T(8,128)(2,1)}, u32[]{:S(2)}) copy-start(bf16[2048,352]{0,1:T(8,128)(2,1)} %param.19) | copy-start | bytes 4325380
  7.2 140.9 %all-gather.2.cloned.1.call-start = ((), (), s32[]{:S(2)}) async-start(), calls=%async_computation.6 | async-start | bytes 14155776 | tf_op jit(solution)/shard_map/all_gather | solution.py:16
  14.5 0.7 copy-start.22
  78.2 75.7 %copy-start.20 = (bf16[1,2048,128]{2,1,0:T(8,128)(2,1)S(1)}, bf16[1,2048,128]{2,1,0:T(8,128)(2,1)}, u32[]{:S(2)}) copy-start(bf16[1,2048,128]{2,1,0:T(8,128)(2,1)} %param.16) | copy-start | bytes 1572868
  78.2 132.9 %reduce-scatter.2.cloned.1.call-start = ((), (), s32[]{:S(2)}) async-start(), calls=%async_computation.7 | async-start | bytes 7077888 | tf_op jit(solution)/shard_map/reduce_scatter | solution.py:190
  153.8 3.8 copy-start.1
  153.8 4.5 copy-start.2
  153.8 1.9 copy-start.21
  155.7 4.7 %copy-start.6 = (f32[1536,128]{1,0:T(8,128)}, f32[1536,128]{1,0:T(8,128)S(1)}, u32[]{:S(2)}) copy-start(f32[1536,128]{1,0:T(8,128)S(1)} %fusion.14) | copy-start | bytes 2359300
  155.7 2.6 copy-start.32
  157.5 2.8 copy-start.8
  160.4 1.8 copy-start.24
  166.6 54.5 %copy-start.27 = (s32[384,2]{0,1:T(2,128)S(1)}, s32[384,2]{0,1:T(2,128)}, u32[]{:S(2)}) copy-start(s32[384,2]{0,1:T(2,128)} %param.14) | copy-start | bytes 9220
  166.6 81.7 %copy-start.23 = (bf16[384,256]{1,0:T(8,128)(2,1)S(1)}, bf16[384,256]{1,0:T(8,128)(2,1)}, u32[]{:S(2)}) copy-start(bf16[384,256]{1,0:T(8,128)(2,1)} %copy-done.22) | copy-start | bytes 589828
  211.0 33.3 %all-to-all-start.1 = ((bf16[32,48,256]{2,1,0:T(8,128)(2,1)}), bf16[32,48,256]{2,1,0:T(8,128)(2,1)S(1)}, u32[]{:S(2)}, u32[]{:S(2)}) async-start(bf16[32,48,256]{2,1,0:T(8,128)(2,1)} %reduce-scatter.2.cloned.1.call-done), calls=%async_computation.2 | async-start | bytes 1572864 | tf_op jit(solution)/shard_map/all_to_all | solution.py:196
  248.4 7.1 %copy-start.26 = (f32[384,352]{0,1:T(8,128)S(1)}, f32[384,352]{0,1:T(8,128)}, u32[]{:S(2)}) copy-start(f32[384,352]{0,1:T(8,128)} %param.21) | copy-start | bytes 1622020
  249.9 32.7 %all-to-all-start.2 = ((bf16[8,384,256]{1,2,0:T(8,128)(2,1)}), bf16[8,384,256]{1,2,0:T(8,128)(2,1)}, u32[]{:S(2)}, u32[]{:S(2)}) async-start(bf16[8,384,256]{1,2,0:T(8,128)(2,1)} %broadcast_in_dim.83), calls=%async_computation.3 | async-start | bytes 3145728 | tf_op jit(solution)/shard_map/all_to_all | solution.py:31
  255.7 140.9 %copy-start.3 = (f32[384,352]{1,0:T(8,128)}, f32[384,352]{1,0:T(8,128)S(1)}, u32[]{:S(2)}) copy-start(f32[384,352]{1,0:T(8,128)S(1)} %copy.108) | copy-start | bytes 1622020
  255.8 0.9 copy-start.19
  262.2 20.4 %copy-start.10 = (bf16[384,352]{1,0:T(8,128)(2,1)}, bf16[384,352]{1,0:T(8,128)(2,1)S(1)}, u32[]{:S(2)}) copy-start(bf16[384,352]{1,0:T(8,128)(2,1)S(1)} %copy.107) | copy-start | bytes 811012
  356.1 17.7 %copy-start.25 = (f32[191,352]{1,0:T(8,128)S(1)}, f32[191,352]{1,0:T(8,128)}, u32[]{:S(2)}) copy-start(f32[191,352]{1,0:T(8,128)} %slice.429) | copy-start | bytes 806788
  359.8 13.8 %copy-start.29 = (f32[1,352]{1,0:T(1,128)S(1)}, f32[1,352]{1,0:T(1,128)}, u32[]{:S(2)}) copy-start(f32[1,352]{1,0:T(1,128)} %slice.509) | copy-start | bytes 4228
  359.8 17.0 %copy-start.28 = (f32[1,352]{1,0:T(1,128)S(1)}, f32[1,352]{1,0:T(1,128)}, u32[]{:S(2)}) copy-start(f32[1,352]{1,0:T(1,128)} %slice.484) | copy-start | bytes 4228
  368.1 14.6 %copy-start.30 = (f32[1,352]{1,0:T(1,128)S(1)}, f32[1,352]{1,0:T(1,128)}, u32[]{:S(2)}) copy-start(f32[1,352]{1,0:T(1,128)} %slice.482) | copy-start | bytes 4228
  382.8 8.3 %copy-start.13 = (f32[384,352]{1,0:T(8,128)}, f32[384,352]{1,0:T(8,128)S(1)}, u32[]{:S(2)}) copy-start(f32[384,352]{1,0:T(8,128)S(1)} %pad.116) | copy-start | bytes 1622020
  384.0 7.1 %copy-start.15 = (f32[384,352]{1,0:T(8,128)}, f32[384,352]{1,0:T(8,128)S(1)}, u32[]{:S(2)}) copy-start(f32[384,352]{1,0:T(8,128)S(1)} %pad.117) | copy-start | bytes 1622020
  391.1 15.5 %all-to-all-start.4 = ((f32[32,2,352]{2,1,0:T(2,128)}), f32[32,2,352]{2,1,0:T(2,128)}, u32[]{:S(2)}, u32[]{:S(2)}) async-start(f32[32,2,352]{2,1,0:T(2,128)} %broadcast_in_dim.85), calls=%async_computation.5 | async-start | bytes 196608 | tf_op jit(solution)/shard_map/all_to_all | solution.py:31
  406.6 10.7 %slice-start = ((s8[6291456]{0:T(1024)(128)(4,1)}), s8[2097152]{0:T(1024)(128)(4,1)S(1)}, s32[]{:S(2)}) async-start(s8[6291456]{0:T(1024)(128)(4,1)} %bitcast.77), calls=%async_computation.8 | async-start | bytes 4194304
  406.6 43.6 %all-to-all-start.3 = ((bf16[32,64,352]{2,1,0:T(8,128)(2,1)}), bf16[32,64,352]{2,1,0:T(8,128)(2,1)}, u32[]{:S(2)}, u32[]{:S(2)}) async-start(bf16[32,64,352]{2,1,0:T(8,128)(2,1)} %bitcast.81), calls=%async_computation.4 | async-start | bytes 3145728 | tf_op jit(solution)/shard_map/all_to_all | solution.py:46
  411.5 5.8 %slice-start.1 = ((s8[6291456]{0:T(1024)(128)(4,1)}), s8[4194304]{0:T(1024)(128)(4,1)S(1)}, s32[]{:S(2)}) async-start(s8[6291456]{0:T(1024)(128)(4,1)} %bitcast.77), calls=%async_computation.9 | async-start | bytes 8388608
  411.5 5.8 %copy-start.7 = (f32[1536,128]{1,0:T(8,128)S(1)}, f32[1536,128]{1,0:T(8,128)}, u32[]{:S(2)}) copy-start(f32[1536,128]{1,0:T(8,128)} %copy-done.6) | copy-start | bytes 2359300
  411.5 5.8 %copy-start.9 = (f32[1536,128]{1,0:T(8,128)S(1)}, f32[1536,128]{1,0:T(8,128)}, u32[]{:S(2)}) copy-start(f32[1536,128]{1,0:T(8,128)} %copy-done.8) | copy-start | bytes 2359300
  417.3 2.1 copy-start.14
  417.3 2.1 copy-start.16
  417.3 3.0 copy-start.17
  417.3 3.0 copy-start.18
  419.4 13.6 %copy-start.31 = (pred[32]{0:T(512)(128)(4,1)S(1)}, pred[32]{0:T(512)(128)(4,1)}, u32[]{:S(2)}) copy-start(pred[32]{0:T(512)(128)(4,1)} %iota_compare_fusion.3) | copy-start | bytes 100
  419.4 14.4 %copy-start.4 = (f32[384,352]{1,0:T(8,128)S(1)}, f32[384,352]{1,0:T(8,128)}, u32[]{:S(2)}) copy-start(f32[384,352]{1,0:T(8,128)} %copy-done.3) | copy-start | bytes 1622020
  419.4 14.4 %copy-start.5 = (f32[384,352]{1,0:T(8,128)S(1)}, f32[384,352]{1,0:T(8,128)}, u32[]{:S(2)}) copy-start(f32[384,352]{1,0:T(8,128)} %copy.109) | copy-start | bytes 1622020
  419.4 14.4 %copy-start.11 = (bf16[384,352]{1,0:T(8,128)(2,1)S(1)}, bf16[384,352]{1,0:T(8,128)(2,1)}, u32[]{:S(2)}) copy-start(bf16[384,352]{1,0:T(8,128)(2,1)} %copy-done.10) | copy-start | bytes 811012
  419.5 14.4 %copy-start.12 = (bf16[384,352]{1,0:T(8,128)(2,1)S(1)}, bf16[384,352]{1,0:T(8,128)(2,1)}, u32[]{:S(2)}) copy-start(bf16[384,352]{1,0:T(8,128)(2,1)} %copy.110) | copy-start | bytes 811012
Sparse Core Ops, SparseCore 0:
  78.3 69.7 all-gather.1
  166.8 44.2 reduce-scatter.1
where the time goes:
time: 464 us; the launch traced here: 459 us
  waiting for transfers between devices  151 us (33%)
  local copies, waits for them, and re-layouts  140 us (30%)
  blocking collectives  51.5 us (11%)
  other arithmetic  44.1 us (10%)
  matrix products  31.4 us (7%)
  starting transfers between devices  26.3 us (6%)
  between operations  15.1 us (3%)
    slice x61, local copies, waits for them, and re-layouts, on_device(): lax.associative_scan(reverse_link, (jnp.flip(following, 0), jnp.flip(dire...  77.6 us
    all_gather x1, waiting for transfers between devices, side_by_side_2(): lax.all_gather(both, axis, axis=dim, tiled=True)  69.7 us
    all_to_all x1, blocking collectives, side_by_side(): lax.all_to_all(both, axis, split_axis=split_dim, concat_axis=concat_dim,...  51.5 us
    reduce_scatter x1, waiting for transfers between devices, on_device(): lax.psum_scatter(partial_value.reshape(groups, capacity, model_width).ast...  44.4 us
    all_to_all x1, waiting for transfers between devices, on_device(): lax.all_to_all(summed, 'sp', split_axis=0, concat_axis=0, tiled=True)  22.9 us
    mul x15, other arithmetic, reverse_link(): return (former[0] * latter[0], latter[0] * former[1] + latter[1])  17.2 us
    unnamed x79, local copies, waits for them, and re-layouts  14.7 us
    all_to_all x2, starting transfers between devices, sent_to_all(): return lax.all_to_all(copies, axis, split_axis=0, concat_axis=0, tiled=True)  11.2 us
  transfers between devices with their start and end apart: 6, of which 5 were waited for; matrix products, arithmetic and copies ran while one was open for 13% of the time, Pallas kernels for 0%

commit v1 on v0

v1 whole, which is shorter than its diff:
```python
import functools
import math

import jax
import jax.numpy as jnp
from jax import lax
from jax.experimental import pallas as pl
from jax.experimental.pallas import tpu as pltpu
from jax.sharding import PartitionSpec as P

F32, BF16 = jnp.float32, jnp.bfloat16
VMEM = pltpu.VMEM
ROOT = math.sqrt(2.0 / math.pi)


def contract(a, b, da, db):
    return lax.dot_general(a, b, (((da,), (db,)), ((), ())), preferred_element_type=F32)


def front_kernel(experts, cap, tp_ref, routes_ref, weight_ref, resid_ref, cot_ref, send_ref, pick_ref, cot_t_ref):
    rows = routes_ref.shape[1]
    width = resid_ref.shape[1]
    r0, r1 = routes_ref[0:1, :], routes_ref[1:2, :]
    w0, w1 = weight_ref[0:1, :], weight_ref[1:2, :]
    ids = lax.broadcasted_iota(jnp.int32, (experts, rows), 0)
    is0, is1 = ids == r0, ids == r1
    named = (jnp.where(is0, 1.0, 0.0) + jnp.where(is1, 1.0, 0.0)).astype(BF16)
    before = lax.broadcasted_iota(jnp.int32, (rows, rows), 0) < lax.broadcasted_iota(jnp.int32, (rows, rows), 1)
    counts = contract(named, jnp.where(before, 1.0, 0.0).astype(BF16), 1, 0)
    slot0 = r0 * cap + jnp.sum(jnp.where(is0, counts, 0.0), axis=0, keepdims=True).astype(jnp.int32)
    slot1 = r1 * cap + jnp.sum(jnp.where(is1, counts, 0.0), axis=0, keepdims=True).astype(jnp.int32)
    resid, cot = resid_ref[...], cot_ref[...]
    part = 8
    for k in range(experts // part):
        size = part * cap
        at = lax.broadcasted_iota(jnp.int32, (size, rows), 0) + k * size
        p0, p1 = at == slot0, at == slot1
        pick = (jnp.where(p0, 1.0, 0.0) + jnp.where(p1, 1.0, 0.0)).astype(BF16)
        pick_ref[k * size : (k + 1) * size, :] = pick
        scale = jnp.sum(jnp.where(p0, w0, 0.0) + jnp.where(p1, w1, 0.0), axis=1, keepdims=True)
        got = contract(pick, resid, 1, 0).astype(BF16)
        cots = (scale * contract(pick, cot, 1, 0)).astype(BF16)
        send_ref[k * part : (k + 1) * part, 0:cap, :] = got.reshape(part, cap, width)
        send_ref[k * part : (k + 1) * part, cap : 2 * cap, :] = cots.reshape(part, cap, width)
    cot_t_ref[...] = cot.astype(F32).T.astype(BF16)


def front(routes_t, weight_t, resid, cotangent, experts, cap, n_tp):
    rows, model = resid.shape
    width = model // n_tp
    tp = lax.axis_index("tp").astype(jnp.int32).reshape(1)
    whole = lambda shape: pl.BlockSpec(shape, lambda i, t: (0,) * len(shape))
    cols = pl.BlockSpec((rows, width), lambda i, t: (0, t[0]))
    return pl.pallas_call(
        functools.partial(front_kernel, experts, cap),
        grid_spec=pltpu.PrefetchScalarGridSpec(
            num_scalar_prefetch=1,
            grid=(1,),
            in_specs=[whole((2, rows)), whole((2, rows)), cols, cols],
            out_specs=[whole((experts, 2 * cap, width)), whole((experts * cap, rows)), whole((width, rows))],
        ),
        out_shape=[
            jax.ShapeDtypeStruct((experts, 2 * cap, width), BF16),
            jax.ShapeDtypeStruct((experts * cap, rows), BF16),
            jax.ShapeDtypeStruct((width, rows), BF16),
        ],
        name="front",
    )(tp, routes_t, weight_t, resid, cotangent)


def shifted(x, by):
    return pltpu.roll(x, x.shape[1] - by, 1)


def reverse_scan(factor, value):
    rows = factor.shape[1]
    lane = lax.broadcasted_iota(jnp.int32, factor.shape, 1)
    by = 1
    while by < rows:
        inside = lane < rows - by
        value = value + factor * jnp.where(inside, shifted(value, by), 0.0)
        factor = factor * jnp.where(inside, shifted(factor, by), 1.0)
        by *= 2
    return factor, value


MESH = pl.DeviceIdType.MESH


def place():
    sp, tp = lax.axis_index("sp"), lax.axis_index("tp")
    z, x, core = lax.div(sp, 4), lax.rem(sp, 4), lax.rem(tp, 2)
    right, left, across = lax.rem(tp + 2, 8), lax.rem(tp + 6, 8), lax.rem(tp + 4, 8)
    return sp, tp, z, x, right, left, across, 1 - 2 * core


def remote(src, dst, send, recv, sp, tp):
    return pltpu.make_async_remote_copy(
        src_ref=src, dst_ref=dst, send_sem=send, recv_sem=recv, device_id={"sp": sp, "tp": tp}, device_id_type=MESH
    )


def greet(peers):
    barrier = pltpu.get_barrier_semaphore()
    for sp, tp in peers:
        pl.semaphore_signal(barrier, inc=1, device_id={"sp": sp, "tp": tp}, device_id_type=MESH)
    return lambda: pl.semaphore_wait(barrier, len(peers))


def tail_kernel(back_ref, pick_ref, cot_t_ref, proj_ref, gate_ref, decay_ref, before_ref, step_ref,
                d_gate_ref, g_step_ref, g_log_ref, g_proj_ref,
                rg, term, from_x, sums, from_z, ends, ends_x, row, ends_z, states, gelu, slope, mixed, dm, prod,
                ag_send, ag_l, ag_r, ag_a, ag_d, x_send, x_recv, z_send, z_recv, e_send, ex_recv, ez_recv):
    sp, tp, z, x, right, left, across, flip = place()
    mate = tp + flip
    channels, rows = gate_ref.shape
    depth = rg.shape[1]
    half_rows = depth // 2
    part = channels // 2
    xs = [z * 4 + lax.rem(x + d, 4) for d in range(1, 4)]
    zs = [lax.rem(z + d, 8) * 4 + x for d in range(1, 8)]
    arrive = greet([(sp, right), (sp, left), (sp, mate)] + [(q, tp) for q in xs + zs])

    slots = pick_ref.shape[0]
    routed = contract(back_ref[...].reshape(slots, depth), pick_ref[...], 0, 0)
    rg[tp] = (cot_t_ref[...].astype(F32) + routed).astype(BF16)
    arrive()

    def half(j, h):
        return rg.at[j, pl.ds(h * half_rows, half_rows), :]

    def moved(ref, k, recv, to):
        return remote(ref, ref, ag_send.at[k], recv, sp, to)

    sent = [
        moved(half(tp, 0), 0, ag_l.at[0], right),
        moved(half(tp, 1), 1, ag_r.at[1], left),
        moved(half(tp, 1), 2, ag_l.at[1], right),
        moved(half(tp, 0), 3, ag_r.at[0], left),
        moved(rg.at[tp], 4, ag_d.at[0], mate),
    ]
    for copy in sent:
        copy.start()

    def prepare(k):
        at = pl.ds(k * part, part)
        v = gate_ref[at, :].astype(F32)
        decays = jnp.exp(decay_ref[at, :])
        state = decays * before_ref[at, :] + step_ref[at, :].astype(F32)
        th = jnp.tanh(ROOT * (v + 0.044715 * (v * v * v)))
        act = 0.5 * v * (1.0 + th)
        gelu[at, :] = act
        states[at, :] = state
        slope[at, :] = 0.5 * (1.0 + th) + 0.5 * v * (1.0 - th * th) * (ROOT * (1.0 + 3.0 * 0.044715 * (v * v)))
        mixed[at, :] = (act * state).astype(BF16)

    def pass_on(ref, k, arrived, recv, to):
        moved(ref, k, arrived, to).wait_recv()
        copy = moved(ref, k, recv, to)
        copy.start()
        sent.append(copy)

    prepare(0)
    pass_on(half(left, 0), 5, ag_l.at[0], ag_a.at[0], right)
    pass_on(half(right, 1), 6, ag_r.at[1], ag_a.at[1], left)
    prepare(1)

    crossing = []

    def use(t, j):
        cols = pl.ds(pl.multiple_of(j * depth, depth), depth)
        piece = rg[j]
        term[j] = contract(piece, mixed[...], 1, 1).astype(BF16).reshape(term.shape[1:])
        for d in range(1, 4):
            to = lax.rem(x + d, 4)
            copy = remote(term.at[j, to], from_x.at[d - 1, j], x_send.at[t, d - 1], x_recv.at[t, d - 1], z * 4 + to, tp)
            copy.start()
            crossing.append(copy)
        product = contract(proj_ref[:, cols], piece, 1, 0)
        dm[...] = product if t == 0 else dm[...] + product

    use(0, tp)
    moved(rg.at[mate], 4, ag_d.at[0], mate).wait_recv()
    use(1, mate)
    moved(half(left, 1), 7, ag_l.at[1], mate).wait_recv()
    copy = moved(rg.at[left], 7, ag_d.at[1], mate)
    copy.start()
    sent.append(copy)
    moved(half(right, 0), 8, ag_r.at[0], mate).wait_recv()
    copy = moved(rg.at[right], 8, ag_d.at[2], mate)
    copy.start()
    sent.append(copy)
    use(2, left)
    use(3, right)
    pass_on(half(across, 0), 9, ag_a.at[0], ag_d.at[3], mate)
    pass_on(half(across, 1), 10, ag_a.at[1], ag_d.at[4], mate)
    moved(rg.at[left + flip], 7, ag_d.at[1], mate).wait_recv()
    use(4, left + flip)
    moved(rg.at[right + flip], 8, ag_d.at[2], mate).wait_recv()
    use(5, right + flip)
    use(6, across)
    moved(half(across + flip, 0), 9, ag_d.at[3], mate).wait_recv()
    moved(half(across + flip, 1), 10, ag_d.at[4], mate).wait_recv()
    use(7, across + flip)
    order = [tp, mate, left, right, left + flip, right + flip, across, across + flip]

    lines = [jnp.zeros((1, channels), F32), jnp.zeros((1, channels), F32)]
    for k in range(2):
        at = pl.ds(k * part, part)
        decays = jnp.exp(decay_ref[at, :])
        d_mixed = dm[at, :]
        d_gate_ref[at, :] = (d_mixed * states[at, :] * slope[at, :]).astype(BF16)
        lane = lax.broadcasted_iota(jnp.int32, decays.shape, 1)
        following = jnp.where(lane < rows - 1, shifted(decays, 1), 1.0)
        products, local = reverse_scan(following, d_mixed * gelu[at, :])
        prod[at, :] = products
        g_step_ref[at, :] = local
        same = lax.broadcasted_iota(jnp.int32, (part, channels), 0) + k * part == lax.broadcasted_iota(
            jnp.int32, (part, channels), 1
        )
        first = decays[:, 0:1]
        for i, ended in enumerate((products, local)):
            lines[i] = lines[i] + jnp.sum(jnp.where(same, first * ended[:, 0:1], 0.0), axis=0, keepdims=True)
    ends[...] = jnp.zeros_like(ends)
    row[...] = jnp.zeros_like(row)
    ends[0:1, :] = lines[0]
    ends[1:2, :] = lines[1]
    ends_x[x] = ends[...]
    passed = []
    for d in range(1, 4):
        copy = remote(ends, ends_x.at[x], e_send.at[d - 1], ex_recv.at[d - 1], z * 4 + lax.rem(x + d, 4), tp)
        copy.start()
        passed.append(copy)

    def cross_sum(t):
        j = order[t]
        total = term[j, x].astype(F32)
        for d in range(1, 4):
            remote(from_x.at[d - 1, j], from_x.at[d - 1, j], x_send.at[t, d - 1], x_recv.at[t, d - 1], sp, mate).wait_recv()
            total = total + from_x[d - 1, j].astype(F32)
        sums[j] = total.astype(BF16)

        @pl.when(j == z)
        def _():
            g_proj_ref[...] = total

        @pl.when(j != z)
        def _():
            remote(sums.at[j], from_z.at[z], z_send.at[j], z_recv.at[z], j * 4 + x, tp).start()

    for t in range(4):
        cross_sum(t)
    scale, shift = jnp.ones((1, channels), F32), jnp.zeros((1, channels), F32)
    for d in range(1, 4):
        q = lax.rem(x + 4 - d, 4)
        remote(ends, ends_x.at[q], e_send.at[d - 1], ex_recv.at[d - 1], sp, mate).wait_recv()
    for q in reversed(range(4)):
        shift = ends_x[q, 1:2, :] + ends_x[q, 0:1, :] * shift
        scale = ends_x[q, 0:1, :] * scale
    row[0:1, :] = scale
    row[1:2, :] = shift
    for d in range(1, 8):
        copy = remote(row, ends_z.at[z], e_send.at[d + 2], ez_recv.at[d - 1], lax.rem(z + d, 8) * 4 + x, tp)
        copy.start()
        passed.append(copy)
    for t in range(4, 8):
        cross_sum(t)
    for d in range(1, 8):
        q = lax.rem(z + 8 - d, 8)
        remote(row, ends_z.at[q], e_send.at[d + 2], ez_recv.at[d - 1], sp, mate).wait_recv()
    ends_z[z] = row[...]
    entering = jnp.zeros((1, channels), F32)
    for q in reversed(range(1, 8)):
        entering = jnp.where(q > z, ends_z[q, 1:2, :] + ends_z[q, 0:1, :] * entering, entering)
    for q in reversed(range(1, 4)):
        entering = jnp.where(q > x, ends_x[q, 1:2, :] + ends_x[q, 0:1, :] * entering, entering)
    for k in range(2):
        at = pl.ds(k * part, part)
        same = lax.broadcasted_iota(jnp.int32, (part, channels), 0) + k * part == lax.broadcasted_iota(
            jnp.int32, (part, channels), 1
        )
        column = jnp.sum(jnp.where(same, entering, 0.0), axis=1, keepdims=True)
        grad = g_step_ref[at, :] + prod[at, :] * column
        g_step_ref[at, :] = grad
        g_log_ref[at, :] = grad * jnp.exp(decay_ref[at, :]) * before_ref[at, :]
    for d in range(1, 8):
        q = lax.rem(z + d, 8)
        remote(from_z.at[q], from_z.at[q], z_send.at[q], z_recv.at[q], sp, mate).wait_recv()
        g_proj_ref[...] += from_z[q].astype(F32)
    for d in range(1, 8):
        q = lax.rem(z + d, 8)
        remote(sums.at[q], from_z.at[z], z_send.at[q], z_recv.at[z], sp, mate).wait_send()
    for copy in sent + crossing + passed:
        copy.wait_send()


def tail(back, pick, cot_t, proj, gate, decay, before, step):
    channels, rows = gate.shape
    depth = cot_t.shape[0]
    flat = (channels, rows)
    lines = 8 * depth // 32
    outs = [(flat, BF16), (flat, F32), (flat, F32), ((lines, channels), F32)]
    dma = pltpu.SemaphoreType.DMA
    return pl.pallas_call(
        tail_kernel,
        in_specs=[pl.BlockSpec(memory_space=VMEM)] * 8,
        out_specs=[pl.BlockSpec(memory_space=VMEM)] * 4,
        out_shape=[jax.ShapeDtypeStruct(s, d) for s, d in outs],
        scratch_shapes=[
            VMEM((8, depth, rows), BF16),
            VMEM((8, 4, lines, channels), BF16),
            VMEM((3, 8, lines, channels), BF16),
            VMEM((8, lines, channels), BF16),
            VMEM((8, lines, channels), BF16),
            VMEM((8, channels), F32),
            VMEM((4, 8, channels), F32),
            VMEM((8, channels), F32),
            VMEM((8, 8, channels), F32),
            VMEM(flat, F32),
            VMEM(flat, F32),
            VMEM(flat, F32),
            VMEM(flat, BF16),
            VMEM(flat, F32),
            VMEM(flat, F32),
            dma((11,)), dma((2,)), dma((2,)), dma((2,)), dma((5,)),
            dma((8, 3)), dma((8, 3)), dma((8,)), dma((8,)), dma((10,)), dma((3,)), dma((7,)),
        ],
        compiler_params=pltpu.CompilerParams(collective_id=1, has_side_effects=True, vmem_limit_bytes=48 << 20),
        name="tail",
    )(back, pick, cot_t, proj, gate, decay, before, step)


def expert_work(in_rows, cot_rows, gate_w, up_w, down_w):
    gate_act = jnp.dot(in_rows, gate_w, preferred_element_type=F32)
    up_act = jnp.dot(in_rows, up_w, preferred_element_type=F32)
    sig = jax.nn.sigmoid(gate_act)
    silu = gate_act * sig
    hidden = (silu * up_act).astype(BF16)
    grad_down = contract(hidden, cot_rows, 0, 0)
    d_hidden = contract(cot_rows, down_w, 1, 1)
    d_gate = (d_hidden * up_act * (sig * (1.0 + gate_act * (1.0 - sig)))).astype(BF16)
    d_up = (d_hidden * silu).astype(BF16)
    grad_gate = contract(in_rows, d_gate, 0, 0)
    grad_up = contract(in_rows, d_up, 0, 0)
    partial_value = contract(d_gate, gate_w, 1, 1) + contract(d_up, up_w, 1, 1)
    return grad_gate[None], grad_up[None], grad_down[None], partial_value.astype(BF16)


def on_device(resid, cotangent, routes, route_weight, w_gate, w_up, w_down, out_proj, gate_pre, log_decay,
              state_before, step_input):
    rows, model = resid.shape
    experts, n_tp = lax.axis_size("sp"), lax.axis_size("tp")
    cap = 2 * rows * routes.shape[1] // experts
    send, pick, cot_t = front(routes.T, route_weight.T, resid, cotangent, experts, cap, n_tp)
    got = lax.all_to_all(send, "sp", split_axis=0, concat_axis=0, tiled=True)
    full = lax.all_gather(got, "tp", axis=2, tiled=True)
    grad_gate, grad_up, grad_down, partial_value = expert_work(
        full[:, :cap].reshape(-1, model), full[:, cap:].reshape(-1, model), w_gate[0], w_up[0], w_down[0]
    )
    summed = lax.psum_scatter(partial_value.reshape(experts, cap, model), "tp", scatter_dimension=2, tiled=True)
    back = lax.all_to_all(summed, "sp", split_axis=0, concat_axis=0, tiled=True)
    d_gate, grad_step, grad_log, grad_proj = tail(
        back, pick, cot_t, out_proj.T, gate_pre.T, log_decay.T, state_before.T, step_input.T
    )
    return grad_gate, grad_up, grad_down, grad_proj, d_gate.T, grad_step.T, grad_log.T


def solution(mesh):
    by_sp, both = P("sp", None), P("sp", "tp")
    cols = P("sp", None, "tp")
    return jax.shard_map(
        on_device,
        mesh=mesh,
        in_specs=(by_sp, by_sp, by_sp, by_sp, cols, cols, P("sp", "tp", None), P(None, "tp"), both, both, both, both),
        out_specs=(cols, cols, P("sp", "tp", None), both, both, both, both),
        check_vma=False,
    )
```

time: 464 us -> 280 us (0.60)
  local copies, waits for them, and re-layouts: 140 us -> 11.4 us
  other arithmetic: 44.1 us -> 0 us
  Pallas kernels: 0 us -> 42.3 us
  waiting for transfers between devices: 151 us -> 121 us
  starting transfers between devices: 26.3 us -> 9.9 us
    slice x85 -> x1, local copies, waits for them, and re-layouts: 85.3 us -> 5.66 us  [on_device(): full[:, cap:].reshape(-1, model)]
    pallas_call x0 -> x2, Pallas kernels: none -> 42.3 us  [the longest x1 38.3 us: tail(): pl.pallas_call(tail_kernel, in_specs=[pl.BlockSpec(memory_space=VMEM)] *...]
    all_to_all x4 -> x1, waiting for transfers between devices: 36.7 us -> 7.13 us  [on_device(): back = lax.all_to_all(summed, 'sp', split_axis=0, concat_axis=0, tiled=True)]
    mul x21 -> x0, other arithmetic: 21.1 us -> none  [the longest x15 17.2 us: reverse_link(): return (former[0] * latter[0], latter[0] * former[1] + latter[1])]
    all_to_all x4 -> x1, starting transfers between devices: 26.1 us -> 9.82 us  [on_device(): back = lax.all_to_all(summed, 'sp', split_axis=0, concat_axis=0, tiled=True)]
    gather x3 -> x0, local copies, waits for them, and re-layouts: 12.2 us -> none  [the longest x1 4.76 us: gather_slots(): cot_pad[slot_token].astype(jnp.float32)]
    rev x2 -> x0, local copies, waits for them, and re-layouts: 10.7 us -> none  [the longest x1 5.36 us: on_device(): local_vals = jnp.flip(local_vals, 0)]
    concatenate x18 -> x0, other arithmetic: 10.5 us -> none  [the longest x15 9.05 us: on_device(): lax.associative_scan(reverse_link, (jnp.flip(following, 0), jnp.flip(dire...]
  transfers between devices with their start and end apart: 6 -> 3, of which waited for: 5 -> 3; matrix products, arithmetic and copies ran while one was open for 13% -> 6% of each run, Pallas kernels for 0% -> 0%
where the time goes in v1:
time: 280 us; the launch traced here: 279 us
  waiting for transfers between devices  121 us (43%)
  blocking collectives  51.8 us (18%)
  Pallas kernels  42.3 us (15%)
  matrix products  28.2 us (10%)
  between operations  14.2 us (5%)
  local copies, waits for them, and re-layouts  11.4 us (4%)
  starting transfers between devices  9.9 us (4%)
    all_gather x1, waiting for transfers between devices, on_device(): full = lax.all_gather(got, 'tp', axis=2, tiled=True)  69.9 us
    all_to_all x1, blocking collectives, on_device(): got = lax.all_to_all(send, 'sp', split_axis=0, concat_axis=0, tiled=True)  51.8 us
    reduce_scatter x1, waiting for transfers between devices, on_device(): lax.psum_scatter(partial_value.reshape(experts, cap, model), 'tp', scatte...  44.4 us
    pallas_call x1, Pallas kernels, tail(): pl.pallas_call(tail_kernel, in_specs=[pl.BlockSpec(memory_space=VMEM)] *...  38.3 us
    dot_general x6, matrix products, contract(): lax.dot_general(a, b, (((da,), (db,)), ((), ())), preferred_element_type=...  24.6 us
    all_to_all x1, starting transfers between devices, on_device(): back = lax.all_to_all(summed, 'sp', split_axis=0, concat_axis=0, tiled=True)  9.82 us
    all_to_all x1, waiting for transfers between devices, on_device(): back = lax.all_to_all(summed, 'sp', split_axis=0, concat_axis=0, tiled=True)  7.13 us
    unnamed x34, local copies, waits for them, and re-layouts  5.76 us
  transfers between devices with their start and end apart: 3, of which 3 were waited for; matrix products, arithmetic and copies ran while one was open for 6% of the time, Pallas kernels for 0%

profile of v1, /device:TPU:16, one launch (start us, length us, event | category | flops | bytes accessed | tf_op | source)
XLA Modules:
  0.0 279.4 jit_solution(16009972106370836743)
XLA Ops:
  7.2 0.0 copy-start
  7.2 0.0 all-gather.2.cloned.1.call-start
  7.2 4.0 %front.1 = (bf16[32,96,256]{2,1,0:T(8,128)(2,1)}, bf16[1536,384]{1,0:T(8,128)(2,1)}, bf16[256,384]{1,0:T(8,128)(2,1)}) custom-call(s32[1]{0:T(128)} %bitcast.tp_ref, s32[2,384]{1,0:T(2,128)} %bitcast.60, f32[2,384]{1,0:T(2,128)} %bitcast.61, bf16[384,2048]{1,0:T(8,128)(2,1)} %resid_ref.1, bf16[384,2048]{1,0:T(8,128)(2,1)} %cot_ref.1), custom_call_target="tpu_custom_call" | custom-call | tf_op jit(solution)/shard_map/front/pallas_call | solution.py:54
  11.3 51.8 %all_to_all.10 = bf16[32,96,256]{2,1,0:T(8,128)(2,1)} all-to-all(bf16[32,96,256]{2,1,0:T(8,128)(2,1)} %get-tuple-element.14), channel_id=1, replica_groups=mesh['sp'=32,'tp'=8] {'sp'}, dimensions={0} | all-to-all | bytes 3145728 | tf_op jit(solution)/shard_map/all_to_all | solution.py:355
  63.1 0.0 all-gather.2.cloned.1.call-update
  63.1 0.0 reduce-scatter.2.cloned.1.call-start
  63.2 69.9 %all-gather.2.cloned.1.call-done = bf16[32,96,2048]{2,1,0:T(8,128)(2,1)} async-done(((bf16[32,96,256]{2,1,0:T(8,128)(2,1)}), bf16[32,96,2048]{2,1,0:T(8,128)(2,1)}) %all-gather.2.cloned.1.call-update) | async-done | bytes 12582928 | tf_op jit(solution)/shard_map/all_gather | solution.py:356
  133.1 5.7 %fusion.12 = (bf16[32,48,2048]{2,1,0:T(8,128)(2,1)S(1)}, bf16[32,48,2048]{2,1,0:T(8,128)(2,1)S(1)}) fusion(bf16[32,96,2048]{2,1,0:T(8,128)(2,1)} %all-gather.2.cloned.1.call-done), kind=kLoop, calls=%fused_computation.19 | loop fusion | bytes 25165824 | tf_op jit(solution)/shard_map/slice | solution.py:358
  138.7 0.0 copy-start.7
  138.8 0.0 copy-start.8
  138.8 0.0 copy-start.13
  138.8 0.0 copy-done
  138.8 1.8 fusion.3
  140.6 0.0 copy-done.13
  140.6 0.0 copy-start.9
  140.6 0.0 copy-start.14
  140.7 1.8 fusion.6
  142.5 0.0 copy-done.7
  142.5 0.0 copy-start.11
  142.5 0.8 copy-done.8
  143.3 0.0 copy-done.14
  143.3 2.0 multiply_convert_fusion.1
  145.3 0.0 copy-done.9
  145.3 0.0 copy-done.11
  145.4 1.8 fusion.1
  147.2 4.4 %add_convert_fusion = bf16[1536,2048]{1,0:T(8,128)(2,1)} fusion(f32[1536,2048]{1,0:T(8,128)S(1)} %fusion.1, bf16[1536,128]{1,0:T(8,128)(2,1)S(1)} %get-tuple-element.23, bf16[1,2048,128]{2,1,0:T(8,128)(2,1)S(1)} %copy-done.13), kind=kOutput, calls=%fused_computation | convolution fusion | flops 811597824 | bytes 19791872 | tf_op jit(solution)/shard_map/dot_general | solution.py:17
  151.6 0.0 reduce-scatter.2.cloned.1.call-update
  151.6 44.4 %reduce-scatter.2.cloned.1.call-done = bf16[32,48,256]{2,1,0:T(8,128)(2,1)} async-done(((bf16[32,48,2048]{2,1,0:T(8,128)(2,1)}), bf16[32,48,256]{2,1,0:T(8,128)(2,1)}) %reduce-scatter.2.cloned.1.call-update) | async-done | bytes 786448 | tf_op jit(solution)/shard_map/reduce_scatter | solution.py:360
  196.0 9.8 %all-to-all-start.1 = ((bf16[32,48,256]{2,1,0:T(8,128)(2,1)}), bf16[32,48,256]{2,1,0:T(8,128)(2,1)S(1)}, u32[]{:S(2)}, u32[]{:S(2)}) async-start(bf16[32,48,256]{2,1,0:T(8,128)(2,1)} %reduce-scatter.2.cloned.1.call-done), calls=%async_computation.2 | async-start | bytes 1572864 | tf_op jit(solution)/shard_map/all_to_all | solution.py:361
  205.8 5.6 %convolution_bitcast_fusion.1 = f32[1,2048,128]{2,1,0:T(8,128)} fusion(bf16[1536,2048]{1,0:T(8,128)(2,1)} %bitcast.54, bf16[1536,128]{1,0:T(8,128)(2,1)S(1)} %get-tuple-element.23), kind=kOutput, calls=%fused_computation.2 | convolution fusion | flops 805306368 | bytes 7733248 | tf_op jit(solution)/shard_map/dot_general | solution.py:17
  211.4 0.0 copy-start.10
  211.4 0.0 copy-start.12
  211.4 5.7 %convolution_bitcast_fusion.2 = f32[1,2048,128]{2,1,0:T(8,128)} fusion(bf16[1536,2048]{1,0:T(8,128)(2,1)} %bitcast.55, bf16[1536,128]{1,0:T(8,128)(2,1)S(1)} %get-tuple-element.24), kind=kOutput, calls=%fused_computation.3 | convolution fusion | flops 805306368 | bytes 7733248 | tf_op jit(solution)/shard_map/dot_general | solution.py:17
  217.1 0.0 copy-done.10
  217.1 0.0 copy-done.12
  217.1 0.0 copy-start.1
  217.1 0.0 copy-start.2
  217.1 0.0 copy-start.4
  217.1 0.0 copy-start.6
  217.2 5.0 %convolution_bitcast_fusion = f32[1,128,2048]{2,1,0:T(8,128)} fusion(bf16[1536,2048]{1,0:T(8,128)(2,1)} %bitcast.58, f32[1536,128]{1,0:T(8,128)S(1)} %copy-done.12, f32[1536,128]{1,0:T(8,128)S(1)} %copy-done.10), kind=kOutput, calls=%fused_computation.1 | convolution fusion | flops 806486016 | bytes 8912896 | tf_op jit(solution)/shard_map/dot_general | solution.py:17
  222.2 7.1 %all-to-all-done.1.back_ref = bf16[32,48,256]{2,1,0:T(8,128)(2,1)S(1)} async-done(((bf16[32,48,256]{2,1,0:T(8,128)(2,1)}), bf16[32,48,256]{2,1,0:T(8,128)(2,1)S(1)}, u32[]{:S(2)}, u32[]{:S(2)}) %all-to-all-start.1) | async-done | bytes 786464 | tf_op jit(solution)/shard_map/all_to_all | solution.py:361
  229.3 0.0 copy-done.1
  229.3 0.0 copy-done.2
  229.3 0.0 copy-done.4
  229.3 0.0 copy-done.6
  229.3 0.0 copy-start.3
  229.3 1.0 copy-done.3
  230.4 0.0 copy-start.5
  230.4 1.0 copy-done.5
  231.3 38.3 %tail.1 = (bf16[352,384]{1,0:T(8,128)(2,1)S(1)}, f32[352,384]{1,0:T(8,128)S(1)}, f32[352,384]{1,0:T(8,128)S(1)}, f32[64,352]{1,0:T(8,128)S(1)}) custom-call(bf16[32,48,256]{2,1,0:T(8,128)(2,1)S(1)} %all-to-all-done.1.back_ref, bf16[1536,384]{1,0:T(8,128)(2,1)S(1)} %copy-done.1, bf16[256,384]{1,0:T(8,128)(2,1)S(1)} %copy-done.6, bf16[352,2048]{1,0:T(8,128)(2,1)} %bitcast.59, ...), custom_call_target="tpu_custom_call" | custom-call | tf_op jit(solution)/shard_map/tail/pallas_call | solution.py:304
  269.6 0.6 copy.23
  270.3 0.7 copy.24
  271.0 0.8 copy.25
  271.8 0.8 copy.26
Async XLA Ops:
  7.2 131.6 %copy-start = (bf16[1,2048,128]{2,1,0:T(8,128)(2,1)S(1)}, bf16[1,2048,128]{2,1,0:T(8,128)(2,1)}, u32[]{:S(2)}) copy-start(bf16[1,2048,128]{2,1,0:T(8,128)(2,1)} %param.16) | copy-start | bytes 1572868
  7.2 125.9 %all-gather.2.cloned.1.call-start = ((), (), s32[]{:S(2)}) async-start(), calls=%async_computation.3 | async-start | bytes 14155776 | tf_op jit(solution)/shard_map/all_gather | solution.py:356
  63.1 132.9 %reduce-scatter.2.cloned.1.call-start = ((), (), s32[]{:S(2)}) async-start(), calls=%async_computation.4 | async-start | bytes 7077888 | tf_op jit(solution)/shard_map/reduce_scatter | solution.py:360
  138.7 3.8 %copy-start.7 = (bf16[32,48,2048]{2,1,0:T(8,128)(2,1)}, bf16[32,48,2048]{2,1,0:T(8,128)(2,1)S(1)}, u32[]{:S(2)}) copy-start(bf16[32,48,2048]{2,1,0:T(8,128)(2,1)S(1)} %get-tuple-element.22) | copy-start | bytes 18874372
  138.8 4.5 %copy-start.8 = (bf16[32,48,2048]{2,1,0:T(8,128)(2,1)}, bf16[32,48,2048]{2,1,0:T(8,128)(2,1)S(1)}, u32[]{:S(2)}) copy-start(bf16[32,48,2048]{2,1,0:T(8,128)(2,1)S(1)} %get-tuple-element.21) | copy-start | bytes 18874372
  138.8 1.9 copy-start.13
  140.6 4.7 %copy-start.9 = (f32[1536,128]{1,0:T(8,128)}, f32[1536,128]{1,0:T(8,128)S(1)}, u32[]{:S(2)}) copy-start(f32[1536,128]{1,0:T(8,128)S(1)} %fusion.3) | copy-start | bytes 2359300
  140.6 2.6 copy-start.14
  142.5 2.8 %copy-start.11 = (f32[1536,128]{1,0:T(8,128)}, f32[1536,128]{1,0:T(8,128)S(1)}, u32[]{:S(2)}) copy-start(f32[1536,128]{1,0:T(8,128)S(1)} %fusion.6) | copy-start | bytes 2359300
  196.0 33.3 %all-to-all-start.1 = ((bf16[32,48,256]{2,1,0:T(8,128)(2,1)}), bf16[32,48,256]{2,1,0:T(8,128)(2,1)S(1)}, u32[]{:S(2)}, u32[]{:S(2)}) async-start(bf16[32,48,256]{2,1,0:T(8,128)(2,1)} %reduce-scatter.2.cloned.1.call-done), calls=%async_computation.2 | async-start | bytes 1572864 | tf_op jit(solution)/shard_map/all_to_all | solution.py:361
  211.4 5.7 %copy-start.10 = (f32[1536,128]{1,0:T(8,128)S(1)}, f32[1536,128]{1,0:T(8,128)}, u32[]{:S(2)}) copy-start(f32[1536,128]{1,0:T(8,128)} %copy-done.9) | copy-start | bytes 2359300
  211.4 5.7 %copy-start.12 = (f32[1536,128]{1,0:T(8,128)S(1)}, f32[1536,128]{1,0:T(8,128)}, u32[]{:S(2)}) copy-start(f32[1536,128]{1,0:T(8,128)} %copy-done.11) | copy-start | bytes 2359300
  217.1 12.2 %copy-start.1 = (bf16[1536,384]{1,0:T(8,128)(2,1)S(1)}, bf16[1536,384]{1,0:T(8,128)(2,1)}, u32[]{:S(2)}) copy-start(bf16[1536,384]{1,0:T(8,128)(2,1)} %get-tuple-element.15.pick_ref) | copy-start | bytes 3538948
  217.1 12.2 %copy-start.2 = (f32[384,352]{0,1:T(8,128)S(1)}, f32[384,352]{0,1:T(8,128)}, u32[]{:S(2)}) copy-start(f32[384,352]{0,1:T(8,128)} %param.21) | copy-start | bytes 1622020
  217.1 12.2 %copy-start.4 = (bf16[384,352]{0,1:T(8,128)(2,1)S(1)}, bf16[384,352]{0,1:T(8,128)(2,1)}, u32[]{:S(2)}) copy-start(bf16[384,352]{0,1:T(8,128)(2,1)} %param.20) | copy-start | bytes 811012
  217.1 12.2 %copy-start.6 = (bf16[256,384]{1,0:T(8,128)(2,1)S(1)}, bf16[256,384]{1,0:T(8,128)(2,1)}, u32[]{:S(2)}) copy-start(bf16[256,384]{1,0:T(8,128)(2,1)} %get-tuple-element.16.cot_t_ref) | copy-start | bytes 589828
  229.3 1.1 copy-start.3
  230.4 1.0 copy-start.5
Sparse Core Ops, SparseCore 0:
  63.2 69.7 all-gather.1
  151.7 44.2 reduce-scatter.1

commit v2 on v1

--- a/solution.py
+++ b/solution.py
@@ -330,20 +330,250 @@
     )(back, pick, cot_t, proj, gate, decay, before, step)
 
 
-def expert_work(in_rows, cot_rows, gate_w, up_w, down_w):
-    gate_act = jnp.dot(in_rows, gate_w, preferred_element_type=F32)
-    up_act = jnp.dot(in_rows, up_w, preferred_element_type=F32)
-    sig = jax.nn.sigmoid(gate_act)
-    silu = gate_act * sig
-    hidden = (silu * up_act).astype(BF16)
-    grad_down = contract(hidden, cot_rows, 0, 0)
-    d_hidden = contract(cot_rows, down_w, 1, 1)
-    d_gate = (d_hidden * up_act * (sig * (1.0 + gate_act * (1.0 - sig)))).astype(BF16)
-    d_up = (d_hidden * silu).astype(BF16)
-    grad_gate = contract(in_rows, d_gate, 0, 0)
-    grad_up = contract(in_rows, d_up, 0, 0)
-    partial_value = contract(d_gate, gate_w, 1, 1) + contract(d_up, up_w, 1, 1)
-    return grad_gate[None], grad_up[None], grad_down[None], partial_value.astype(BF16)
+N_SENDS = 13
+
+
+def experts_kernel(send_ref, w_gate_ref, w_up_ref, w_down_ref,
+                   g_gate_ref, g_up_ref, g_down_ref, back_ref,
+                   buf, w_cat, w_cat_t, w_down_t, acc_t, parts, from_mate, pair, from_far, from_left, from_right, ret, back,
+                   a_send, a_recv, sends, yl, yr, ya, ym, pm, fa, fl, fr, b_send, b_recv):
+    sp, tp, z, x, right, left, across, flip = place()
+    mate = tp + flip
+    core = lax.rem(tp, 2)
+    y = lax.div(tp, 2)
+    y_right, y_left, y_far = lax.rem(y + 1, 4), lax.rem(y + 3, 4), lax.rem(y + 2, 4)
+    n_sp, both_caps, depth = send_ref.shape
+    cap = both_caps // 2
+    steps = n_sp // 4
+    arrive = greet([(lax.rem(sp + k, n_sp), tp) for k in range(1, n_sp)] + [(sp, right), (sp, left), (sp, mate)])
+
+    def dz(s):
+        h = lax.div(s + 1, 2)
+        return lax.rem(jnp.where(lax.rem(s, 2) == 1, h, steps - h), steps)
+
+    def group(s):
+        return lax.rem(z + dz(s), steps)
+
+    def toward(s, d):
+        return lax.rem(z - dz(s) + steps, steps) * 4 + lax.rem(x + d, 4)
+
+    def out_copy(s, d):
+        to = toward(s, d)
+        return remote(send_ref.at[to], buf.at[tp, sp], a_send.at[s, d], a_recv.at[s, d], to, tp)
+
+    def back_copy(s, d):
+        to = group(s) * 4 + lax.rem(x + d, 4)
+        return remote(ret.at[to], back.at[sp], b_send.at[s, d], b_recv.at[s, d], to, tp)
+
+    arrive()
+    pltpu.make_async_copy(send_ref.at[sp], buf.at[tp, sp], a_recv.at[0, 0]).start()
+    for d in range(1, 4):
+        out_copy(0, d).start()
+
+    @pl.loop(1, steps)
+    def _(s):
+        for d in range(4):
+            out_copy(s, d).start()
+
+    def wait(ref, sem):
+        remote(ref, ref, a_send.at[0, 0], sem, sp, mate).wait_recv()
+
+    w_cat[:, 0:128] = w_gate_ref[...]
+    w_cat[:, 128:256] = w_up_ref[...]
+    acc_t[...] = jnp.zeros_like(acc_t)
+    g_down_ref[...] = jnp.zeros_like(g_down_ref)
+
+    @pl.loop(0, 8)
+    def _(j):
+        at = pl.ds(pl.multiple_of(j * depth, depth), depth)
+        w_cat_t[:, at] = w_cat[at, :].astype(F32).T.astype(BF16)
+        w_down_t[at, :] = w_down_ref[:, at].astype(F32).T.astype(BF16)
+
+    def four(s):
+        return pl.ds(group(s) * 4, 4)
+
+    def two(s, h):
+        return pl.ds(group(s) * 4 + 2 * h, 2)
+
+    def sends_of(s, first, last):
+        blk = four(s)
+        makers = [
+            lambda: remote(buf.at[tp, blk], buf.at[tp, blk], sends.at[s, 0], yl.at[s], sp, right),
+            lambda: remote(buf.at[tp, blk], buf.at[tp, blk], sends.at[s, 1], yr.at[s], sp, left),
+            lambda: remote(buf.at[tp, blk], buf.at[tp, blk], sends.at[s, 2], ym.at[s, 0], sp, mate),
+            lambda: remote(buf.at[left, two(s, 0)], buf.at[left, two(s, 0)], sends.at[s, 3], ya.at[s, 0], sp, right),
+            lambda: remote(buf.at[right, two(s, 1)], buf.at[right, two(s, 1)], sends.at[s, 4], ya.at[s, 1], sp, left),
+            lambda: remote(buf.at[left, blk], buf.at[left, blk], sends.at[s, 5], ym.at[s, 1], sp, mate),
+            lambda: remote(buf.at[right, blk], buf.at[right, blk], sends.at[s, 6], ym.at[s, 2], sp, mate),
+            lambda: remote(buf.at[across, blk], buf.at[across, blk], sends.at[s, 7], ym.at[s, 3], sp, mate),
+            lambda: remote(parts.at[1 - core, :, blk], from_mate.at[:, blk], sends.at[s, 8], pm.at[s], sp, mate),
+            lambda: remote(pair.at[y_far, two(s, 0)], from_far.at[two(s, 0)], sends.at[s, 9], fa.at[s, 0], sp, right),
+            lambda: remote(pair.at[y_far, two(s, 1)], from_far.at[two(s, 1)], sends.at[s, 10], fa.at[s, 1], sp, left),
+            lambda: remote(pair.at[y_right, blk], from_left.at[blk], sends.at[s, 11], fl.at[s], sp, right),
+            lambda: remote(pair.at[y_left, blk], from_right.at[blk], sends.at[s, 12], fr.at[s], sp, left),
+        ]
+        return [make() for make in makers[first:last]]
+
+    def spread(s):
+        for d in range(4):
+            q = group(s) * 4 + lax.rem(x + 4 - d, 4)
+            wait(buf.at[tp, q], a_recv.at[s, d])
+        for copy in sends_of(s, 0, 3):
+            copy.start()
+
+    def forward(s):
+        wait(buf.at[left, four(s)], yl.at[s])
+        wait(buf.at[right, four(s)], yr.at[s])
+        for copy in sends_of(s, 3, 7):
+            copy.start()
+
+    def hand_over(s):
+        wait(buf.at[across, two(s, 0)], ya.at[s, 0])
+        wait(buf.at[across, two(s, 1)], ya.at[s, 1])
+        sends_of(s, 7, 8)[0].start()
+
+    def compute(s):
+        blk = four(s)
+        for k, j in enumerate((tp, left, right, across)):
+            wait(buf.at[j + flip, blk], ym.at[s, k])
+        size = 4 * cap
+
+        def rows_of(j):
+            return buf[j, blk, 0:cap, :].reshape(size, depth)
+
+        def cots_of(j):
+            return buf[j, blk, cap : 2 * cap, :].reshape(size, depth)
+
+        act = jnp.zeros((size, 256), F32)
+        d_hidden = jnp.zeros((size, 128), F32)
+        for j in range(8):
+            cols = slice(j * depth, (j + 1) * depth)
+            act = act + contract(rows_of(j), w_cat[cols, :], 1, 0)
+            d_hidden = d_hidden + contract(cots_of(j), w_down_t[cols, :], 1, 0)
+        gate_act, up_act = act[:, 0:128], act[:, 128:256]
+        sig = jax.nn.sigmoid(gate_act)
+        silu = gate_act * sig
+        hidden = (silu * up_act).astype(BF16)
+        d_gate = (d_hidden * up_act * (sig * (1.0 + gate_act * (1.0 - sig)))).astype(BF16)
+        d_up = (d_hidden * silu).astype(BF16)
+        d_both = jnp.concatenate([d_gate, d_up], axis=1)
+        d_both_t = d_both.astype(F32).T.astype(BF16)
+        hidden_t = hidden.astype(F32).T.astype(BF16)
+        for j in range(8):
+            cols = slice(j * depth, (j + 1) * depth)
+            value = contract(d_both, w_cat_t[:, cols], 1, 0).astype(BF16)
+            parts[j % 2, j // 2, blk] = value.reshape(4, cap, depth)
+        sends_of(s, 8, 9)[0].start()
+        for j in range(8):
+            cols = slice(j * depth, (j + 1) * depth)
+            acc_t[:, cols] += contract(d_both_t, rows_of(j), 1, 0)
+            g_down_ref[:, cols] += contract(hidden_t, cots_of(j), 1, 0)
+
+    def pair_up(s):
+        blk = four(s)
+        wait(from_mate.at[:, blk], pm.at[s])
+        for k in range(4):
+            pair[k, blk] = (parts[core, k, blk].astype(F32) + from_mate[k, blk].astype(F32)).astype(BF16)
+        for copy in sends_of(s, 9, 11):
+            copy.start()
+
+    def join(s):
+        wait(from_far.at[two(s, 0)], fa.at[s, 0])
+        wait(from_far.at[two(s, 1)], fa.at[s, 1])
+        for k, h in ((y_right, 0), (y_left, 1)):
+            at = two(s, h)
+            pair[k, at] = (pair[k, at].astype(F32) + from_far[at].astype(F32)).astype(BF16)
+        for copy in sends_of(s, 11, 13):
+            copy.start()
+
+    def finish(s):
+        blk = four(s)
+        wait(from_left.at[blk], fl.at[s])
+        wait(from_right.at[blk], fr.at[s])
+        ret[blk] = (pair[y, blk].astype(F32) + from_left[blk].astype(F32) + from_right[blk].astype(F32)).astype(BF16)
+
+        @pl.when(s == 0)
+        def _():
+            pltpu.make_async_copy(ret.at[sp], back.at[sp], b_recv.at[0, 0]).start()
+
+        @pl.when(s > 0)
+        def _():
+            back_copy(s, 0).start()
+
+        for d in range(1, 4):
+            back_copy(s, d).start()
+
+    stages = ((spread, 0), (forward, 1), (hand_over, 2), (finish, 6), (join, 5), (pair_up, 4), (compute, 3))
+
+    @pl.loop(0, steps + 6)
+    def _(t):
+        for stage, late in stages:
+            @pl.when((t >= late) & (t < steps + late))
+            def _():
+                stage(t - late)
+
+    for j in range(8):
+        cols = slice(j * depth, (j + 1) * depth)
+        both = acc_t[:, cols].T
+        g_gate_ref[cols, :] = both[:, 0:128]
+        g_up_ref[cols, :] = both[:, 128:256]
+
+    @pl.loop(0, steps)
+    def _(s):
+        for d in range(4):
+            q = lax.rem(z - dz(s) + steps, steps) * 4 + lax.rem(x + 4 - d, 4)
+            wait(back.at[q], b_recv.at[s, d])
+
+    back_ref[...] = back[...]
+
+    @pl.loop(0, steps)
+    def _(s):
+        for copy in sends_of(s, 0, N_SENDS):
+            copy.wait_send()
+        for d in range(1, 4):
+            out_copy(s, d).wait_send()
+            back_copy(s, d).wait_send()
+
+        @pl.when(s > 0)
+        def _():
+            out_copy(s, 0).wait_send()
+            back_copy(s, 0).wait_send()
+
+
+def experts_pass(send, w_gate, w_up, w_down):
+    n_sp, both_caps, depth = send.shape
+    model, units = w_gate.shape
+    cap = both_caps // 2
+    block = (n_sp, cap, depth)
+    steps = n_sp // 4
+    dma = pltpu.SemaphoreType.DMA
+    outs = [((model, units), F32), ((model, units), F32), ((units, model), F32), (block, BF16)]
+    return pl.pallas_call(
+        experts_kernel,
+        in_specs=[pl.BlockSpec(memory_space=VMEM)] * 4,
+        out_specs=[pl.BlockSpec(memory_space=VMEM)] * 4,
+        out_shape=[jax.ShapeDtypeStruct(s, d) for s, d in outs],
+        scratch_shapes=[
+            VMEM((8, n_sp, both_caps, depth), BF16),
+            VMEM((model, 2 * units), BF16),
+            VMEM((2 * units, model), BF16),
+            VMEM((model, units), BF16),
+            VMEM((2 * units, model), F32),
+            VMEM((2, 4, *block), BF16),
+            VMEM((4, *block), BF16),
+            VMEM((4, *block), BF16),
+            VMEM(block, BF16),
+            VMEM(block, BF16),
+            VMEM(block, BF16),
+            VMEM(block, BF16),
+            VMEM(block, BF16),
+            dma((steps, 4)), dma((steps, 4)), dma((steps, N_SENDS)),
+            dma((steps,)), dma((steps,)), dma((steps, 2)), dma((steps, 4)), dma((steps,)), dma((steps, 2)),
+            dma((steps,)), dma((steps,)), dma((steps, 4)), dma((steps, 4)),
+        ],
+        compiler_params=pltpu.CompilerParams(collective_id=0, has_side_effects=True, vmem_limit_bytes=60 << 20),
+        name="experts",
+    )(send, w_gate, w_up, w_down)
 
 
 def on_device(resid, cotangent, routes, route_weight, w_gate, w_up, w_down, out_proj, gate_pre, log_decay,
@@ -352,17 +582,11 @@
     experts, n_tp = lax.axis_size("sp"), lax.axis_size("tp")
     cap = 2 * rows * routes.shape[1] // experts
     send, pick, cot_t = front(routes.T, route_weight.T, resid, cotangent, experts, cap, n_tp)
-    got = lax.all_to_all(send, "sp", split_axis=0, concat_axis=0, tiled=True)
-    full = lax.all_gather(got, "tp", axis=2, tiled=True)
-    grad_gate, grad_up, grad_down, partial_value = expert_work(
-        full[:, :cap].reshape(-1, model), full[:, cap:].reshape(-1, model), w_gate[0], w_up[0], w_down[0]
-    )
-    summed = lax.psum_scatter(partial_value.reshape(experts, cap, model), "tp", scatter_dimension=2, tiled=True)
-    back = lax.all_to_all(summed, "sp", split_axis=0, concat_axis=0, tiled=True)
+    grad_gate, grad_up, grad_down, back = experts_pass(send, w_gate[0], w_up[0], w_down[0])
     d_gate, grad_step, grad_log, grad_proj = tail(
         back, pick, cot_t, out_proj.T, gate_pre.T, log_decay.T, state_before.T, step_input.T
     )
-    return grad_gate, grad_up, grad_down, grad_proj, d_gate.T, grad_step.T, grad_log.T
+    return grad_gate[None], grad_up[None], grad_down[None], grad_proj, d_gate.T, grad_step.T, grad_log.T
 
 
 def solution(mesh):

time: 280 us -> 171 us (0.61)
  waiting for transfers between devices: 121 us -> 0 us
  Pallas kernels: 42.3 us -> 162 us
  blocking collectives: 51.8 us -> 0 us
  matrix products: 28.2 us -> 0 us
  between operations: 14.2 us -> 0.76 us
  starting transfers between devices: 9.9 us -> 0 us
  local copies, waits for them, and re-layouts: 11.4 us -> 8.26 us
    pallas_call x0 -> x1, Pallas kernels: none -> 118 us  [experts_pass(): pl.pallas_call(experts_kernel, in_specs=[pl.BlockSpec(memory_space=VMEM)]...]
    all_gather x1 -> x0, waiting for transfers between devices: 69.9 us -> none  [on_device(): full = lax.all_gather(got, 'tp', axis=2, tiled=True)]
    all_to_all x1 -> x0, blocking collectives: 51.8 us -> none  [on_device(): got = lax.all_to_all(send, 'sp', split_axis=0, concat_axis=0, tiled=True)]
    reduce_scatter x1 -> x0, waiting for transfers between devices: 44.4 us -> none  [on_device(): lax.psum_scatter(partial_value.reshape(experts, cap, model), 'tp', scatte...]
    dot_general x8 -> x0, matrix products: 28.2 us -> none  [the longest x6 24.6 us: contract(): lax.dot_general(a, b, (((da,), (db,)), ((), ())), preferred_element_type=...]
    all_to_all x1 -> x0, starting transfers between devices: 9.82 us -> none  [on_device(): back = lax.all_to_all(summed, 'sp', split_axis=0, concat_axis=0, tiled=True)]
    all_to_all x1 -> x0, waiting for transfers between devices: 7.13 us -> none  [on_device(): back = lax.all_to_all(summed, 'sp', split_axis=0, concat_axis=0, tiled=True)]
    slice x1 -> x0, local copies, waits for them, and re-layouts: 5.66 us -> none  [on_device(): full[:, cap:].reshape(-1, model)]
  transfers between devices with their start and end apart: 3 -> 0, of which waited for: 3 -> 0; matrix products, arithmetic and copies ran while one was open for 6% -> 0% of each run, Pallas kernels for 0% -> 0%
where the time goes in v2:
time: 171 us
  Pallas kernels  162 us (95%)
  local copies, waits for them, and re-layouts  8.26 us (5%)
    pallas_call x1, Pallas kernels, experts_pass(): pl.pallas_call(experts_kernel, in_specs=[pl.BlockSpec(memory_space=VMEM)]...  118 us
    pallas_call x1, Pallas kernels, tail(): pl.pallas_call(tail_kernel, in_specs=[pl.BlockSpec(memory_space=VMEM)] *...  40.2 us
    unnamed x27, local copies, waits for them, and re-layouts  8.26 us
    pallas_call x1, Pallas kernels, front(): pl.pallas_call(functools.partial(front_kernel, experts, cap), grid_spec=p...  4.01 us

profile of v2, /device:TPU:16, one launch (start us, length us, event | category | flops | bytes accessed | tf_op | source)
XLA Modules:
  0.0 171.1 jit_solution(3255018680230414233)
XLA Ops:
  0.6 4.0 %front.1 = (bf16[32,96,256]{2,1,0:T(8,128)(2,1)}, bf16[1536,384]{1,0:T(8,128)(2,1)}, bf16[256,384]{1,0:T(8,128)(2,1)}) custom-call(s32[1]{0:T(128)} %bitcast.tp_ref, s32[2,384]{1,0:T(2,128)} %bitcast.31, f32[2,384]{1,0:T(2,128)} %bitcast.32, bf16[384,2048]{1,0:T(8,128)(2,1)} %resid_ref.1, bf16[384,2048]{1,0:T(8,128)(2,1)} %cot_ref.1), custom_call_target="tpu_custom_call" | custom-call | tf_op jit(solution)/shard_map/front/pallas_call | solution.py:54
  4.6 0.0 copy-start
  4.7 0.0 copy-start.2
  4.7 0.0 copy-start.3
  4.7 0.0 copy-start.4
  4.7 0.0 copy-start.5
  4.7 0.0 copy-start.6
  4.7 117.9 %experts.1 = (f32[2048,128]{1,0:T(8,128)}, f32[2048,128]{1,0:T(8,128)}, f32[128,2048]{1,0:T(8,128)}, bf16[32,48,256]{2,1,0:T(8,128)(2,1)}) custom-call(bf16[32,96,256]{2,1,0:T(8,128)(2,1)} %get-tuple-element.18.send_ref, bf16[2048,128]{1,0:T(8,128)(2,1)} %bitcast.28, bf16[2048,128]{1,0:T(8,128)(2,1)} %bitcast.29, bf16[128,2048]{1,0:T(8,128)(2,1)} %bitcast.30), custom_call_target="tpu_custom_call" | custom-call | tf_op jit(solution)/shard_map/experts/pallas_call | solution.py:551
  122.6 0.0 copy-done
  122.6 0.0 copy-done.2
  122.6 0.0 copy-done.3
  122.6 0.0 copy-done.4
  122.6 0.0 copy-done.5
  122.6 0.0 copy-done.6
  122.6 0.0 copy-start.1
  122.7 1.1 copy-done.1
  123.8 0.0 copy-start.9
  123.8 40.2 %tail.1 = (bf16[352,384]{1,0:T(8,128)(2,1)S(1)}, f32[352,384]{1,0:T(8,128)S(1)}, f32[352,384]{1,0:T(8,128)S(1)}, f32[64,352]{1,0:T(8,128)S(1)}) custom-call(bf16[32,48,256]{2,1,0:T(8,128)(2,1)S(1)} %copy-done.1, bf16[1536,384]{1,0:T(8,128)(2,1)S(1)} %copy-done, bf16[256,384]{1,0:T(8,128)(2,1)S(1)} %copy-done.6, bf16[352,2048]{1,0:T(8,128)(2,1)} %bitcast.24, ...), custom_call_target="tpu_custom_call" | custom-call | tf_op jit(solution)/shard_map/tail/pallas_call | solution.py:304
  164.0 0.0 copy-start.8
  164.0 0.0 copy-done.9
  164.0 1.0 copy.26
  165.0 0.6 copy-done.8
  165.6 0.0 copy-start.7
  165.6 1.0 copy.27
  166.6 0.6 copy-done.7
  167.2 1.0 copy.28
  168.2 0.6 copy.29
  168.8 0.7 copy.30
  169.5 0.8 copy.31
  170.3 0.8 copy.32
Async XLA Ops:
  4.6 117.9 %copy-start = (bf16[1536,384]{1,0:T(8,128)(2,1)S(1)}, bf16[1536,384]{1,0:T(8,128)(2,1)}, u32[]{:S(2)}) copy-start(bf16[1536,384]{1,0:T(8,128)(2,1)} %get-tuple-element.23.pick_ref) | copy-start | bytes 3538948
  4.7 117.9 %copy-start.2 = (f32[384,352]{0,1:T(8,128)S(1)}, f32[384,352]{0,1:T(8,128)}, u32[]{:S(2)}) copy-start(f32[384,352]{0,1:T(8,128)} %param.21) | copy-start | bytes 1622020
  4.7 118.0 %copy-start.3 = (f32[384,352]{0,1:T(8,128)S(1)}, f32[384,352]{0,1:T(8,128)}, u32[]{:S(2)}) copy-start(f32[384,352]{0,1:T(8,128)} %param.22) | copy-start | bytes 1622020
  4.7 118.0 %copy-start.4 = (bf16[384,352]{0,1:T(8,128)(2,1)S(1)}, bf16[384,352]{0,1:T(8,128)(2,1)}, u32[]{:S(2)}) copy-start(bf16[384,352]{0,1:T(8,128)(2,1)} %param.20) | copy-start | bytes 811012
  4.7 118.0 %copy-start.5 = (bf16[384,352]{0,1:T(8,128)(2,1)S(1)}, bf16[384,352]{0,1:T(8,128)(2,1)}, u32[]{:S(2)}) copy-start(bf16[384,352]{0,1:T(8,128)(2,1)} %param.23) | copy-start | bytes 811012
  4.7 118.0 %copy-start.6 = (bf16[256,384]{1,0:T(8,128)(2,1)S(1)}, bf16[256,384]{1,0:T(8,128)(2,1)}, u32[]{:S(2)}) copy-start(bf16[256,384]{1,0:T(8,128)(2,1)} %get-tuple-element.24.cot_t_ref) | copy-start | bytes 589828
  122.6 1.1 copy-start.1
  123.8 40.2 %copy-start.9 = (f32[2048,128]{1,0:T(8,128)S(1)}, f32[2048,128]{1,0:T(8,128)}, u32[]{:S(2)}) copy-start(f32[2048,128]{1,0:T(8,128)} %get-tuple-element.19) | copy-start | bytes 3145732
  164.0 1.6 copy-start.8
  165.6 1.6 copy-start.7

commit v3 on v2

--- a/solution.py
+++ b/solution.py
@@ -17,7 +17,8 @@
     return lax.dot_general(a, b, (((da,), (db,)), ((), ())), preferred_element_type=F32)
 
 
-def front_kernel(experts, cap, tp_ref, routes_ref, weight_ref, resid_ref, cot_ref, send_ref, pick_ref, cot_t_ref):
+def front_kernel(experts, cap, tp_ref, routes_ref, weight_ref, resid_ref, cot_ref, resid_far_ref, cot_far_ref,
+                 send_ref, pick_ref, cot_t_ref):
     rows = routes_ref.shape[1]
     width = resid_ref.shape[1]
     r0, r1 = routes_ref[0:1, :], routes_ref[1:2, :]
@@ -29,7 +30,6 @@
     counts = contract(named, jnp.where(before, 1.0, 0.0).astype(BF16), 1, 0)
     slot0 = r0 * cap + jnp.sum(jnp.where(is0, counts, 0.0), axis=0, keepdims=True).astype(jnp.int32)
     slot1 = r1 * cap + jnp.sum(jnp.where(is1, counts, 0.0), axis=0, keepdims=True).astype(jnp.int32)
-    resid, cot = resid_ref[...], cot_ref[...]
     part = 8
     for k in range(experts // part):
         size = part * cap
@@ -38,34 +38,38 @@
         pick = (jnp.where(p0, 1.0, 0.0) + jnp.where(p1, 1.0, 0.0)).astype(BF16)
         pick_ref[k * size : (k + 1) * size, :] = pick
         scale = jnp.sum(jnp.where(p0, w0, 0.0) + jnp.where(p1, w1, 0.0), axis=1, keepdims=True)
-        got = contract(pick, resid, 1, 0).astype(BF16)
-        cots = (scale * contract(pick, cot, 1, 0)).astype(BF16)
-        send_ref[k * part : (k + 1) * part, 0:cap, :] = got.reshape(part, cap, width)
-        send_ref[k * part : (k + 1) * part, cap : 2 * cap, :] = cots.reshape(part, cap, width)
-    cot_t_ref[...] = cot.astype(F32).T.astype(BF16)
+        at = slice(k * part, (k + 1) * part)
+        for i, (resid, cot) in enumerate(((resid_ref, cot_ref), (resid_far_ref, cot_far_ref))):
+            got = contract(pick, resid[...], 1, 0).astype(BF16)
+            cots = (scale * contract(pick, cot[...], 1, 0)).astype(BF16)
+            send_ref[i, at, 0:cap, :] = got.reshape(part, cap, width)
+            send_ref[i, at, cap : 2 * cap, :] = cots.reshape(part, cap, width)
+    cot_t_ref[...] = cot_ref[...].astype(F32).T.astype(BF16)
 
 
 def front(routes_t, weight_t, resid, cotangent, experts, cap, n_tp):
     rows, model = resid.shape
     width = model // n_tp
-    tp = lax.axis_index("tp").astype(jnp.int32).reshape(1)
+    tp = lax.axis_index("tp").astype(jnp.int32)
+    slices = jnp.stack([tp, lax.rem(tp + n_tp // 2, n_tp)])
     whole = lambda shape: pl.BlockSpec(shape, lambda i, t: (0,) * len(shape))
     cols = pl.BlockSpec((rows, width), lambda i, t: (0, t[0]))
+    far = pl.BlockSpec((rows, width), lambda i, t: (0, t[1]))
     return pl.pallas_call(
         functools.partial(front_kernel, experts, cap),
         grid_spec=pltpu.PrefetchScalarGridSpec(
             num_scalar_prefetch=1,
             grid=(1,),
-            in_specs=[whole((2, rows)), whole((2, rows)), cols, cols],
-            out_specs=[whole((experts, 2 * cap, width)), whole((experts * cap, rows)), whole((width, rows))],
+            in_specs=[whole((2, rows)), whole((2, rows)), cols, cols, far, far],
+            out_specs=[whole((2, experts, 2 * cap, width)), whole((experts * cap, rows)), whole((width, rows))],
         ),
         out_shape=[
-            jax.ShapeDtypeStruct((experts, 2 * cap, width), BF16),
+            jax.ShapeDtypeStruct((2, experts, 2 * cap, width), BF16),
             jax.ShapeDtypeStruct((experts * cap, rows), BF16),
             jax.ShapeDtypeStruct((width, rows), BF16),
         ],
         name="front",
-    )(tp, routes_t, weight_t, resid, cotangent)
+    )(slices, routes_t, weight_t, resid, cotangent, resid, cotangent)
 
 
 def shifted(x, by):
@@ -330,50 +334,69 @@
     )(back, pick, cot_t, proj, gate, decay, before, step)
 
 
-N_SENDS = 13
+N_SENDS = 14
+ORDER = (0, 1, 3, 5, 4, 2, 6, 7)
+FAR = (2, 5)
 
 
 def experts_kernel(send_ref, w_gate_ref, w_up_ref, w_down_ref,
-                   g_gate_ref, g_up_ref, g_down_ref, back_ref,
-                   buf, w_cat, w_cat_t, w_down_t, acc_t, parts, from_mate, pair, from_far, from_left, from_right, ret, back,
-                   a_send, a_recv, sends, yl, yr, ya, ym, pm, fa, fl, fr, b_send, b_recv):
+                   acc_t, g_down_ref, back_ref,
+                   buf, w_cat, w_cat_t, w_down_t, parts, from_mate, pair, from_far, from_left, from_right, ret, back,
+                   a_send, a_recv, far_send, far_recv, sends, yl, yr, ya, ym, pm, fa, fl, fr, b_send, b_recv):
     sp, tp, z, x, right, left, across, flip = place()
     mate = tp + flip
     core = lax.rem(tp, 2)
     y = lax.div(tp, 2)
     y_right, y_left, y_far = lax.rem(y + 1, 4), lax.rem(y + 3, 4), lax.rem(y + 2, 4)
-    n_sp, both_caps, depth = send_ref.shape
+    n_sp, both_caps, depth = send_ref.shape[1:]
     cap = both_caps // 2
-    steps = n_sp // 4
+    n_z = n_sp // 4
+    steps = 2 * n_z
     arrive = greet([(lax.rem(sp + k, n_sp), tp) for k in range(1, n_sp)] + [(sp, right), (sp, left), (sp, mate)])
 
-    def dz(s):
-        h = lax.div(s + 1, 2)
-        return lax.rem(jnp.where(lax.rem(s, 2) == 1, h, steps - h), steps)
-
-    def group(s):
-        return lax.rem(z + dz(s), steps)
-
-    def toward(s, d):
-        return lax.rem(z - dz(s) + steps, steps) * 4 + lax.rem(x + d, 4)
-
-    def out_copy(s, d):
-        to = toward(s, d)
-        return remote(send_ref.at[to], buf.at[tp, sp], a_send.at[s, d], a_recv.at[s, d], to, tp)
-
-    def back_copy(s, d):
-        to = group(s) * 4 + lax.rem(x + d, 4)
-        return remote(ret.at[to], back.at[sp], b_send.at[s, d], b_recv.at[s, d], to, tp)
+    def dz(i):
+        found = 0
+        for k, value in enumerate(ORDER):
+            found = jnp.where(i == k, value, found)
+        return found
+
+    def source(i):
+        return lax.rem(z + dz(i), n_z) * 4
+
+    def target(i):
+        return lax.rem(z - dz(i) + n_z, n_z) * 4
+
+    def is_far(i):
+        return (i >= FAR[0]) & (i < FAR[1])
+
+    def out_copy(i, d):
+        to = target(i) + lax.rem(x + d, 4)
+        return remote(send_ref.at[0, to], buf.at[tp, sp], a_send.at[i, d], a_recv.at[i, x], to, tp)
+
+    def out_far(i, d):
+        to = target(i) + lax.rem(x + d, 4)
+        return remote(send_ref.at[1, to], buf.at[across, sp], far_send.at[i, d], far_recv.at[i, x], to, tp)
+
+    def back_copy(i, q):
+        to = source(i) + q
+        return remote(ret.at[to], back.at[sp], b_send.at[i, q], b_recv.at[i, x], to, tp)
 
     arrive()
-    pltpu.make_async_copy(send_ref.at[sp], buf.at[tp, sp], a_recv.at[0, 0]).start()
+    pltpu.make_async_copy(send_ref.at[0, sp], buf.at[tp, sp], a_recv.at[0, x]).start()
+    pltpu.make_async_copy(send_ref.at[1, sp], buf.at[across, sp], far_recv.at[0, x]).start()
     for d in range(1, 4):
         out_copy(0, d).start()
-
-    @pl.loop(1, steps)
-    def _(s):
+        out_far(0, d).start()
+
+    @pl.loop(1, n_z)
+    def _(i):
         for d in range(4):
-            out_copy(s, d).start()
+            out_copy(i, d).start()
+
+        @pl.when(jnp.logical_not(is_far(i)))
+        def _():
+            for d in range(4):
+                out_far(i, d).start()
 
     def wait(ref, sem):
         remote(ref, ref, a_send.at[0, 0], sem, sp, mate).wait_recv()
@@ -389,54 +412,76 @@
         w_cat_t[:, at] = w_cat[at, :].astype(F32).T.astype(BF16)
         w_down_t[at, :] = w_down_ref[:, at].astype(F32).T.astype(BF16)
 
-    def four(s):
-        return pl.ds(group(s) * 4, 4)
-
-    def two(s, h):
-        return pl.ds(group(s) * 4 + 2 * h, 2)
-
-    def sends_of(s, first, last):
-        blk = four(s)
+    def first(s):
+        return source(lax.div(s, 2)) + 2 * lax.rem(s, 2)
+
+    def far(s):
+        return is_far(lax.div(s, 2))
+
+    def sends_of(s, *which):
+        at = first(s)
+        blk = pl.ds(at, 2)
+
+        def same(j, to, k, recv):
+            return remote(buf.at[j, blk], buf.at[j, blk], sends.at[s, k], recv, sp, to)
+
         makers = [
-            lambda: remote(buf.at[tp, blk], buf.at[tp, blk], sends.at[s, 0], yl.at[s], sp, right),
-            lambda: remote(buf.at[tp, blk], buf.at[tp, blk], sends.at[s, 1], yr.at[s], sp, left),
-            lambda: remote(buf.at[tp, blk], buf.at[tp, blk], sends.at[s, 2], ym.at[s, 0], sp, mate),
-            lambda: remote(buf.at[left, two(s, 0)], buf.at[left, two(s, 0)], sends.at[s, 3], ya.at[s, 0], sp, right),
-            lambda: remote(buf.at[right, two(s, 1)], buf.at[right, two(s, 1)], sends.at[s, 4], ya.at[s, 1], sp, left),
-            lambda: remote(buf.at[left, blk], buf.at[left, blk], sends.at[s, 5], ym.at[s, 1], sp, mate),
-            lambda: remote(buf.at[right, blk], buf.at[right, blk], sends.at[s, 6], ym.at[s, 2], sp, mate),
-            lambda: remote(buf.at[across, blk], buf.at[across, blk], sends.at[s, 7], ym.at[s, 3], sp, mate),
+            lambda: same(tp, right, 0, yl.at[s]),
+            lambda: same(tp, left, 1, yr.at[s]),
+            lambda: same(tp, mate, 2, ym.at[s, 0]),
+            lambda: remote(buf.at[left, at], buf.at[left, at], sends.at[s, 3], ya.at[s, 0], sp, right),
+            lambda: remote(buf.at[right, at + 1], buf.at[right, at + 1], sends.at[s, 4], ya.at[s, 1], sp, left),
+            lambda: same(left, mate, 5, ym.at[s, 1]),
+            lambda: same(right, mate, 6, ym.at[s, 2]),
+            lambda: same(across, mate, 7, ym.at[s, 3]),
             lambda: remote(parts.at[1 - core, :, blk], from_mate.at[:, blk], sends.at[s, 8], pm.at[s], sp, mate),
-            lambda: remote(pair.at[y_far, two(s, 0)], from_far.at[two(s, 0)], sends.at[s, 9], fa.at[s, 0], sp, right),
-            lambda: remote(pair.at[y_far, two(s, 1)], from_far.at[two(s, 1)], sends.at[s, 10], fa.at[s, 1], sp, left),
+            lambda: remote(pair.at[y_far, at], from_far.at[at], sends.at[s, 9], fa.at[s, 0], sp, right),
+            lambda: remote(pair.at[y_far, at + 1], from_far.at[at + 1], sends.at[s, 10], fa.at[s, 1], sp, left),
             lambda: remote(pair.at[y_right, blk], from_left.at[blk], sends.at[s, 11], fl.at[s], sp, right),
             lambda: remote(pair.at[y_left, blk], from_right.at[blk], sends.at[s, 12], fr.at[s], sp, left),
         ]
-        return [make() for make in makers[first:last]]
+        return [makers[k]() for k in which]
+
+    def start(s, *which):
+        for copy in sends_of(s, *which):
+            copy.start()
 
     def spread(s):
-        for d in range(4):
-            q = group(s) * 4 + lax.rem(x + 4 - d, 4)
-            wait(buf.at[tp, q], a_recv.at[s, d])
-        for copy in sends_of(s, 0, 3):
-            copy.start()
+        i, q = lax.div(s, 2), 2 * lax.rem(s, 2)
+        at = first(s)
+        for k in range(2):
+            wait(buf.at[tp, at + k], a_recv.at[i, q + k])
+        start(s, 0, 1, 2)
+
+        @pl.when(jnp.logical_not(far(s)))
+        def _():
+            for k in range(2):
+                wait(buf.at[across, at + k], far_recv.at[i, q + k])
+            start(s, 7)
 
     def forward(s):
-        wait(buf.at[left, four(s)], yl.at[s])
-        wait(buf.at[right, four(s)], yr.at[s])
-        for copy in sends_of(s, 3, 7):
-            copy.start()
+        blk = pl.ds(first(s), 2)
+        wait(buf.at[left, blk], yl.at[s])
+        wait(buf.at[right, blk], yr.at[s])
+
+        @pl.when(far(s))
+        def _():
+            start(s, 3, 4)
+
+        start(s, 5, 6)
 
     def hand_over(s):
-        wait(buf.at[across, two(s, 0)], ya.at[s, 0])
-        wait(buf.at[across, two(s, 1)], ya.at[s, 1])
-        sends_of(s, 7, 8)[0].start()
+        @pl.when(far(s))
+        def _():
+            wait(buf.at[across, first(s)], ya.at[s, 0])
+            wait(buf.at[across, first(s) + 1], ya.at[s, 1])
+            start(s, 7)
 
     def compute(s):
-        blk = four(s)
+        blk = pl.ds(first(s), 2)
         for k, j in enumerate((tp, left, right, across)):
             wait(buf.at[j + flip, blk], ym.at[s, k])
-        size = 4 * cap
+        size = 2 * cap
 
         def rows_of(j):
             return buf[j, blk, 0:cap, :].reshape(size, depth)
@@ -462,46 +507,42 @@
         for j in range(8):
             cols = slice(j * depth, (j + 1) * depth)
             value = contract(d_both, w_cat_t[:, cols], 1, 0).astype(BF16)
-            parts[j % 2, j // 2, blk] = value.reshape(4, cap, depth)
-        sends_of(s, 8, 9)[0].start()
+            parts[j % 2, j // 2, blk] = value.reshape(2, cap, depth)
+        start(s, 8)
         for j in range(8):
             cols = slice(j * depth, (j + 1) * depth)
             acc_t[:, cols] += contract(d_both_t, rows_of(j), 1, 0)
             g_down_ref[:, cols] += contract(hidden_t, cots_of(j), 1, 0)
 
     def pair_up(s):
-        blk = four(s)
+        blk = pl.ds(first(s), 2)
         wait(from_mate.at[:, blk], pm.at[s])
         for k in range(4):
             pair[k, blk] = (parts[core, k, blk].astype(F32) + from_mate[k, blk].astype(F32)).astype(BF16)
-        for copy in sends_of(s, 9, 11):
-            copy.start()
+        start(s, 9, 10)
 
     def join(s):
-        wait(from_far.at[two(s, 0)], fa.at[s, 0])
-        wait(from_far.at[two(s, 1)], fa.at[s, 1])
+        at = first(s)
         for k, h in ((y_right, 0), (y_left, 1)):
-            at = two(s, h)
-            pair[k, at] = (pair[k, at].astype(F32) + from_far[at].astype(F32)).astype(BF16)
-        for copy in sends_of(s, 11, 13):
-            copy.start()
+            wait(from_far.at[at + h], fa.at[s, h])
+            pair[k, at + h] = (pair[k, at + h].astype(F32) + from_far[at + h].astype(F32)).astype(BF16)
+        start(s, 11, 12)
 
     def finish(s):
-        blk = four(s)
+        i, q = lax.div(s, 2), 2 * lax.rem(s, 2)
+        at = first(s)
+        blk = pl.ds(at, 2)
         wait(from_left.at[blk], fl.at[s])
         wait(from_right.at[blk], fr.at[s])
         ret[blk] = (pair[y, blk].astype(F32) + from_left[blk].astype(F32) + from_right[blk].astype(F32)).astype(BF16)
-
-        @pl.when(s == 0)
-        def _():
-            pltpu.make_async_copy(ret.at[sp], back.at[sp], b_recv.at[0, 0]).start()
-
-        @pl.when(s > 0)
-        def _():
-            back_copy(s, 0).start()
-
-        for d in range(1, 4):
-            back_copy(s, d).start()
+        for k in range(2):
+            @pl.when(at + k == sp)
+            def _():
+                pltpu.make_async_copy(ret.at[sp], back.at[sp], b_recv.at[0, x]).start()
+
+            @pl.when(at + k != sp)
+            def _():
+                back_copy(i, q + k).start()
 
     stages = ((spread, 0), (forward, 1), (hand_over, 2), (finish, 6), (join, 5), (pair_up, 4), (compute, 3))
 
@@ -512,53 +553,58 @@
             def _():
                 stage(t - late)
 
-    for j in range(8):
-        cols = slice(j * depth, (j + 1) * depth)
-        both = acc_t[:, cols].T
-        g_gate_ref[cols, :] = both[:, 0:128]
-        g_up_ref[cols, :] = both[:, 128:256]
+    @pl.loop(0, n_z)
+    def _(i):
+        for q in range(4):
+            wait(back.at[target(i) + q], b_recv.at[i, q])
+
+    back_ref[...] = back[...]
 
     @pl.loop(0, steps)
     def _(s):
+        for copy in sends_of(s, 0, 1, 2, 5, 6, 7, 8, 9, 10, 11, 12):
+            copy.wait_send()
+
+        @pl.when(far(s))
+        def _():
+            for copy in sends_of(s, 3, 4):
+                copy.wait_send()
+
+    @pl.loop(0, n_z)
+    def _(i):
         for d in range(4):
-            q = lax.rem(z - dz(s) + steps, steps) * 4 + lax.rem(x + 4 - d, 4)
-            wait(back.at[q], b_recv.at[s, d])
-
-    back_ref[...] = back[...]
-
-    @pl.loop(0, steps)
-    def _(s):
-        for copy in sends_of(s, 0, N_SENDS):
-            copy.wait_send()
-        for d in range(1, 4):
-            out_copy(s, d).wait_send()
-            back_copy(s, d).wait_send()
-
-        @pl.when(s > 0)
-        def _():
-            out_copy(s, 0).wait_send()
-            back_copy(s, 0).wait_send()
+            @pl.when(target(i) + lax.rem(x + d, 4) != sp)
+            def _():
+                out_copy(i, d).wait_send()
+
+                @pl.when(jnp.logical_not(is_far(i)))
+                def _():
+                    out_far(i, d).wait_send()
+
+            @pl.when(source(i) + d != sp)
+            def _():
+                back_copy(i, d).wait_send()
 
 
 def experts_pass(send, w_gate, w_up, w_down):
-    n_sp, both_caps, depth = send.shape
+    _, n_sp, both_caps, depth = send.shape
     model, units = w_gate.shape
     cap = both_caps // 2
     block = (n_sp, cap, depth)
-    steps = n_sp // 4
+    n_z = n_sp // 4
+    steps = 2 * n_z
     dma = pltpu.SemaphoreType.DMA
-    outs = [((model, units), F32), ((model, units), F32), ((units, model), F32), (block, BF16)]
+    outs = [((2 * units, model), F32), ((units, model), F32), (block, BF16)]
     return pl.pallas_call(
         experts_kernel,
         in_specs=[pl.BlockSpec(memory_space=VMEM)] * 4,
-        out_specs=[pl.BlockSpec(memory_space=VMEM)] * 4,
+        out_specs=[pl.BlockSpec(memory_space=VMEM)] * 3,
         out_shape=[jax.ShapeDtypeStruct(s, d) for s, d in outs],
         scratch_shapes=[
             VMEM((8, n_sp, both_caps, depth), BF16),
             VMEM((model, 2 * units), BF16),
             VMEM((2 * units, model), BF16),
             VMEM((model, units), BF16),
-            VMEM((2 * units, model), F32),
             VMEM((2, 4, *block), BF16),
             VMEM((4, *block), BF16),
             VMEM((4, *block), BF16),
@@ -567,13 +613,44 @@
             VMEM(block, BF16),
             VMEM(block, BF16),
             VMEM(block, BF16),
-            dma((steps, 4)), dma((steps, 4)), dma((steps, N_SENDS)),
+            dma((n_z, 4)), dma((n_z, 4)), dma((n_z, 4)), dma((n_z, 4)), dma((steps, N_SENDS)),
             dma((steps,)), dma((steps,)), dma((steps, 2)), dma((steps, 4)), dma((steps,)), dma((steps, 2)),
-            dma((steps,)), dma((steps,)), dma((steps, 4)), dma((steps, 4)),
+            dma((steps,)), dma((steps,)), dma((n_z, 4)), dma((n_z, 4)),
         ],
         compiler_params=pltpu.CompilerParams(collective_id=0, has_side_effects=True, vmem_limit_bytes=60 << 20),
         name="experts",
     )(send, w_gate, w_up, w_down)
+
+
+def settle_kernel(acc_ref, down_in, gate_in, step_in, log_in, proj_in, g_gate, g_up, g_down, d_gate, g_step, g_log, g_proj):
+    both = acc_ref[...].T
+    units = g_gate.shape[1]
+    g_gate[...] = both[:, 0:units]
+    g_up[...] = both[:, units : 2 * units]
+    for src, dst in ((down_in, g_down), (gate_in, d_gate), (step_in, g_step), (log_in, g_log), (proj_in, g_proj)):
+        dst[...] = src[...]
+
+
+def settle(acc_t, g_down, d_gate, g_step, g_log, g_proj):
+    parts = 4
+    units, model = g_down.shape
+
+    def rows(a):
+        return pl.BlockSpec((a.shape[0] // parts, a.shape[1]), lambda i: (i, 0))
+
+    def cols(a):
+        return pl.BlockSpec((a.shape[0], a.shape[1] // parts), lambda i: (0, i))
+
+    tall = jax.ShapeDtypeStruct((model, units), F32)
+    rest = [d_gate, g_step, g_log, g_proj]
+    return pl.pallas_call(
+        settle_kernel,
+        grid=(parts,),
+        in_specs=[cols(acc_t), cols(g_down)] + [rows(a) for a in rest],
+        out_specs=[rows(tall), rows(tall), cols(g_down)] + [rows(a) for a in rest],
+        out_shape=[tall, tall] + [jax.ShapeDtypeStruct(a.shape, a.dtype) for a in [g_down] + rest],
+        name="settle",
+    )(acc_t, g_down, *rest)
 
 
 def on_device(resid, cotangent, routes, route_weight, w_gate, w_up, w_down, out_proj, gate_pre, log_decay,
@@ -582,10 +659,9 @@
     experts, n_tp = lax.axis_size("sp"), lax.axis_size("tp")
     cap = 2 * rows * routes.shape[1] // experts
     send, pick, cot_t = front(routes.T, route_weight.T, resid, cotangent, experts, cap, n_tp)
-    grad_gate, grad_up, grad_down, back = experts_pass(send, w_gate[0], w_up[0], w_down[0])
-    d_gate, grad_step, grad_log, grad_proj = tail(
-        back, pick, cot_t, out_proj.T, gate_pre.T, log_decay.T, state_before.T, step_input.T
-    )
+    acc_t, grad_down, back = experts_pass(send, w_gate[0], w_up[0], w_down[0])
+    ended = tail(back, pick, cot_t, out_proj.T, gate_pre.T, log_decay.T, state_before.T, step_input.T)
+    grad_gate, grad_up, grad_down, d_gate, grad_step, grad_log, grad_proj = settle(acc_t, grad_down, *ended)
     return grad_gate[None], grad_up[None], grad_down[None], grad_proj, d_gate.T, grad_step.T, grad_log.T
 
 

time: 171 us -> 182 us (1.064)
  Pallas kernels: 162 us -> 176 us
  local copies, waits for them, and re-layouts: 8.26 us -> 4.14 us
    pallas_call x1, Pallas kernels: 118 us -> 124 us  [experts_pass(): pl.pallas_call(experts_kernel, in_specs=[pl.BlockSpec(memory_space=VMEM)]...]
    pallas_call x0 -> x1, Pallas kernels: none -> 4.94 us  [settle(): pl.pallas_call(settle_kernel, grid=(parts,), in_specs=[cols(acc_t), cols(...]
    unnamed x27 -> x22, local copies, waits for them, and re-layouts: 8.26 us -> 4.14 us
    pallas_call x1, Pallas kernels: 4.01 us -> 6.13 us  [front(): pl.pallas_call(functools.partial(front_kernel, experts, cap), grid_spec=p...]
where the time goes in v3:
time: 182 us; the launch traced here: 181 us
  Pallas kernels  176 us (97%)
  local copies, waits for them, and re-layouts  4.14 us (2%)
    pallas_call x1, Pallas kernels, experts_pass(): pl.pallas_call(experts_kernel, in_specs=[pl.BlockSpec(memory_space=VMEM)]...  124 us
    pallas_call x1, Pallas kernels, tail(): pl.pallas_call(tail_kernel, in_specs=[pl.BlockSpec(memory_space=VMEM)] *...  40.8 us
    pallas_call x1, Pallas kernels, front(): pl.pallas_call(functools.partial(front_kernel, experts, cap), grid_spec=p...  6.13 us
    pallas_call x1, Pallas kernels, settle(): pl.pallas_call(settle_kernel, grid=(parts,), in_specs=[cols(acc_t), cols(...  4.94 us
    unnamed x22, local copies, waits for them, and re-layouts  4.14 us

profile of v3, /device:TPU:16, one launch (start us, length us, event | category | flops | bytes accessed | tf_op | source)
XLA Modules:
  0.0 181.4 jit_solution(17433203413725948662)
XLA Ops:
  0.6 0.6 pad_add_fusion.tp_ref
  1.2 6.1 %front.1 = (bf16[2,32,96,256]{3,2,1,0:T(8,128)(2,1)}, bf16[1536,384]{1,0:T(8,128)(2,1)}, bf16[256,384]{1,0:T(8,128)(2,1)}) custom-call(s32[2]{0:T(128)} %pad_add_fusion.tp_ref, s32[2,384]{1,0:T(2,128)} %bitcast.26, f32[2,384]{1,0:T(2,128)} %bitcast.27, bf16[384,2048]{1,0:T(8,128)(2,1)} %resid_far_ref.1, bf16[384,2048]{1,0:T(8,128)(2,1)} %cot_far_ref.1, ...), custom_call_target="tpu_custom_call" | custom-call | tf_op jit(solution)/shard_map/front/pallas_call | solution.py:58
  7.4 0.0 copy-start
  7.4 0.0 copy-start.2
  7.4 0.0 copy-start.3
  7.4 0.0 copy-start.6
  7.4 0.0 copy-start.7
  7.4 0.0 copy-start.9
  7.4 123.9 %experts.1 = (f32[256,2048]{1,0:T(8,128)}, f32[128,2048]{1,0:T(8,128)}, bf16[32,48,256]{2,1,0:T(8,128)(2,1)}) custom-call(bf16[2,32,96,256]{3,2,1,0:T(8,128)(2,1)} %get-tuple-element.24.send_ref, bf16[2048,128]{1,0:T(8,128)(2,1)} %bitcast.23, bf16[2048,128]{1,0:T(8,128)(2,1)} %bitcast.24, bf16[128,2048]{1,0:T(8,128)(2,1)} %bitcast.25), custom_call_target="tpu_custom_call" | custom-call | tf_op jit(solution)/shard_map/experts/pallas_call | solution.py:598
  131.3 0.0 copy-done
  131.3 0.0 copy-done.2
  131.3 0.0 copy-done.3
  131.3 0.0 copy-done.6
  131.4 0.0 copy-done.7
  131.4 0.0 copy-done.9
  131.4 0.0 copy-start.1
  131.4 1.1 copy-done.1
  132.5 40.8 %tail.1 = (bf16[352,384]{1,0:T(8,128)(2,1)S(1)}, f32[352,384]{1,0:T(8,128)S(1)}, f32[352,384]{1,0:T(8,128)S(1)}, f32[64,352]{1,0:T(8,128)S(1)}) custom-call(bf16[32,48,256]{2,1,0:T(8,128)(2,1)S(1)} %copy-done.1, bf16[1536,384]{1,0:T(8,128)(2,1)S(1)} %copy-done, bf16[256,384]{1,0:T(8,128)(2,1)S(1)} %copy-done.9, bf16[352,2048]{1,0:T(8,128)(2,1)} %bitcast.22, ...), custom_call_target="tpu_custom_call" | custom-call | tf_op jit(solution)/shard_map/tail/pallas_call | solution.py:308
  173.4 0.0 copy-start.4
  173.4 0.8 copy-done.4
  174.2 0.0 copy-start.5
  174.2 0.8 copy-done.5
  175.0 0.0 copy-start.8
  175.0 0.7 copy-done.8
  175.7 0.0 copy-start.10
  175.7 0.6 copy-done.10
  176.3 4.9 %settle.1 = (f32[2048,128]{1,0:T(8,128)}, f32[2048,128]{1,0:T(8,128)}, f32[128,2048]{1,0:T(8,128)}, bf16[352,384]{1,0:T(8,128)(2,1)}, f32[352,384]{1,0:T(8,128)}, /*index=5*/f32[352,384]{1,0:T(8,128)}, f32[64,352]{1,0:T(8,128)}) custom-call(f32[256,2048]{1,0:T(8,128)} %get-tuple-element.25.acc_ref, f32[128,2048]{1,0:T(8,128)} %get-tuple-element.26.down_in, ...), custom_call_target="tpu_custom_call" | custom-call | tf_op jit(solution)/shard_map/settle/pallas_call | solution.py:646
Async XLA Ops:
  7.4 124.0 %copy-start = (bf16[1536,384]{1,0:T(8,128)(2,1)S(1)}, bf16[1536,384]{1,0:T(8,128)(2,1)}, u32[]{:S(2)}) copy-start(bf16[1536,384]{1,0:T(8,128)(2,1)} %get-tuple-element.28.pick_ref) | copy-start | bytes 3538948
  7.4 124.0 %copy-start.2 = (f32[384,352]{0,1:T(8,128)S(1)}, f32[384,352]{0,1:T(8,128)}, u32[]{:S(2)}) copy-start(f32[384,352]{0,1:T(8,128)} %param.21) | copy-start | bytes 1622020
  7.4 124.0 %copy-start.3 = (f32[384,352]{0,1:T(8,128)S(1)}, f32[384,352]{0,1:T(8,128)}, u32[]{:S(2)}) copy-start(f32[384,352]{0,1:T(8,128)} %param.22) | copy-start | bytes 1622020
  7.4 124.0 %copy-start.6 = (bf16[384,352]{0,1:T(8,128)(2,1)S(1)}, bf16[384,352]{0,1:T(8,128)(2,1)}, u32[]{:S(2)}) copy-start(bf16[384,352]{0,1:T(8,128)(2,1)} %param.20) | copy-start | bytes 811012
  7.4 124.0 %copy-start.7 = (bf16[384,352]{0,1:T(8,128)(2,1)S(1)}, bf16[384,352]{0,1:T(8,128)(2,1)}, u32[]{:S(2)}) copy-start(bf16[384,352]{0,1:T(8,128)(2,1)} %param.23) | copy-start | bytes 811012
  7.4 124.0 %copy-start.9 = (bf16[256,384]{1,0:T(8,128)(2,1)S(1)}, bf16[256,384]{1,0:T(8,128)(2,1)}, u32[]{:S(2)}) copy-start(bf16[256,384]{1,0:T(8,128)(2,1)} %get-tuple-element.29.cot_t_ref) | copy-start | bytes 589828
  131.4 1.1 copy-start.1
  173.4 0.8 copy-start.4
  174.2 0.8 copy-start.5
  175.0 0.7 copy-start.8
  175.7 0.6 copy-start.10

commit v4 on v3

--- a/solution.py
+++ b/solution.py
@@ -68,6 +68,7 @@
             jax.ShapeDtypeStruct((experts * cap, rows), BF16),
             jax.ShapeDtypeStruct((width, rows), BF16),
         ],
+        compiler_params=pltpu.CompilerParams(vmem_limit_bytes=24 << 20),
         name="front",
     )(slices, routes_t, weight_t, resid, cotangent, resid, cotangent)
 
@@ -329,7 +330,7 @@
             dma((11,)), dma((2,)), dma((2,)), dma((2,)), dma((5,)),
             dma((8, 3)), dma((8, 3)), dma((8,)), dma((8,)), dma((10,)), dma((3,)), dma((7,)),
         ],
-        compiler_params=pltpu.CompilerParams(collective_id=1, has_side_effects=True, vmem_limit_bytes=48 << 20),
+        compiler_params=pltpu.CompilerParams(collective_id=1, has_side_effects=True, vmem_limit_bytes=24 << 20),
         name="tail",
     )(back, pick, cot_t, proj, gate, decay, before, step)
 
@@ -340,8 +341,8 @@
 
 
 def experts_kernel(send_ref, w_gate_ref, w_up_ref, w_down_ref,
-                   acc_t, g_down_ref, back_ref,
-                   buf, w_cat, w_cat_t, w_down_t, parts, from_mate, pair, from_far, from_left, from_right, ret, back,
+                   g_gate_ref, g_up_ref, g_down_ref, back_ref,
+                   buf, w_cat, w_cat_t, w_down, w_down_t, acc_t, acc_down, g_tall, loads, stores, parts, from_mate, pair, from_far, from_left, from_right, ret, back,
                    a_send, a_recv, far_send, far_recv, sends, yl, yr, ya, ym, pm, fa, fl, fr, b_send, b_recv):
     sp, tp, z, x, right, left, across, flip = place()
     mate = tp + flip
@@ -381,6 +382,11 @@
         to = source(i) + q
         return remote(ret.at[to], back.at[sp], b_send.at[i, q], b_recv.at[i, x], to, tp)
 
+    weights = [
+        pltpu.make_async_copy(w_gate_ref, w_cat.at[:, 0:128], loads.at[0]),
+        pltpu.make_async_copy(w_up_ref, w_cat.at[:, 128:256], loads.at[1]),
+        pltpu.make_async_copy(w_down_ref, w_down, loads.at[2]),
+    ]
     arrive()
     pltpu.make_async_copy(send_ref.at[0, sp], buf.at[tp, sp], a_recv.at[0, x]).start()
     pltpu.make_async_copy(send_ref.at[1, sp], buf.at[across, sp], far_recv.at[0, x]).start()
@@ -401,16 +407,21 @@
     def wait(ref, sem):
         remote(ref, ref, a_send.at[0, 0], sem, sp, mate).wait_recv()
 
-    w_cat[:, 0:128] = w_gate_ref[...]
-    w_cat[:, 128:256] = w_up_ref[...]
-    acc_t[...] = jnp.zeros_like(acc_t)
-    g_down_ref[...] = jnp.zeros_like(g_down_ref)
-
-    @pl.loop(0, 8)
-    def _(j):
-        at = pl.ds(pl.multiple_of(j * depth, depth), depth)
-        w_cat_t[:, at] = w_cat[at, :].astype(F32).T.astype(BF16)
-        w_down_t[at, :] = w_down_ref[:, at].astype(F32).T.astype(BF16)
+    for copy in weights:
+        copy.start()
+
+    def prepare(t):
+        @pl.when(t == 0)
+        def _():
+            for copy in weights:
+                copy.wait()
+            acc_t[...] = jnp.zeros_like(acc_t)
+            acc_down[...] = jnp.zeros_like(acc_down)
+
+        for k in range(2):
+            at = pl.ds(pl.multiple_of((2 * t + k) * depth, depth), depth)
+            w_cat_t[:, at] = w_cat[at, :].astype(F32).T.astype(BF16)
+            w_down_t[at, :] = w_down[:, at].astype(F32).T.astype(BF16)
 
     def first(s):
         return source(lax.div(s, 2)) + 2 * lax.rem(s, 2)
@@ -512,7 +523,7 @@
         for j in range(8):
             cols = slice(j * depth, (j + 1) * depth)
             acc_t[:, cols] += contract(d_both_t, rows_of(j), 1, 0)
-            g_down_ref[:, cols] += contract(hidden_t, cots_of(j), 1, 0)
+            acc_down[:, cols] += contract(hidden_t, cots_of(j), 1, 0)
 
     def pair_up(s):
         blk = pl.ds(first(s), 2)
@@ -544,21 +555,40 @@
             def _():
                 back_copy(i, q + k).start()
 
-    stages = ((spread, 0), (forward, 1), (hand_over, 2), (finish, 6), (join, 5), (pair_up, 4), (compute, 3))
-
-    @pl.loop(0, steps + 6)
+    stages = ((spread, 0), (forward, 2), (hand_over, 4), (finish, 10), (join, 8), (pair_up, 6), (compute, 5))
+
+    @pl.loop(0, steps + 10)
     def _(t):
         for stage, late in stages:
             @pl.when((t >= late) & (t < steps + late))
             def _():
                 stage(t - late)
 
+        @pl.when(t < 4)
+        def _():
+            prepare(t)
+
+    for j in range(8):
+        cols = slice(j * depth, (j + 1) * depth)
+        both = acc_t[:, cols].T
+        g_tall[0, cols, :] = both[:, 0:128]
+        g_tall[1, cols, :] = both[:, 128:256]
+    results = [
+        pltpu.make_async_copy(g_tall.at[0], g_gate_ref, stores.at[0]),
+        pltpu.make_async_copy(g_tall.at[1], g_up_ref, stores.at[1]),
+        pltpu.make_async_copy(acc_down, g_down_ref, stores.at[2]),
+    ]
+    for copy in results:
+        copy.start()
+
     @pl.loop(0, n_z)
     def _(i):
         for q in range(4):
             wait(back.at[target(i) + q], b_recv.at[i, q])
 
     back_ref[...] = back[...]
+    for copy in results:
+        copy.wait()
 
     @pl.loop(0, steps)
     def _(s):
@@ -594,17 +624,22 @@
     n_z = n_sp // 4
     steps = 2 * n_z
     dma = pltpu.SemaphoreType.DMA
-    outs = [((2 * units, model), F32), ((units, model), F32), (block, BF16)]
+    outs = [((model, units), F32), ((model, units), F32), ((units, model), F32), (block, BF16)]
     return pl.pallas_call(
         experts_kernel,
-        in_specs=[pl.BlockSpec(memory_space=VMEM)] * 4,
-        out_specs=[pl.BlockSpec(memory_space=VMEM)] * 3,
+        in_specs=[pl.BlockSpec(memory_space=pl.ANY)] * 4,
+        out_specs=[pl.BlockSpec(memory_space=pl.ANY)] * 3 + [pl.BlockSpec(memory_space=VMEM)],
         out_shape=[jax.ShapeDtypeStruct(s, d) for s, d in outs],
         scratch_shapes=[
             VMEM((8, n_sp, both_caps, depth), BF16),
             VMEM((model, 2 * units), BF16),
             VMEM((2 * units, model), BF16),
+            VMEM((units, model), BF16),
             VMEM((model, units), BF16),
+            VMEM((2 * units, model), F32),
+            VMEM((units, model), F32),
+            VMEM((2, model, units), F32),
+            dma((3,)), dma((3,)),
             VMEM((2, 4, *block), BF16),
             VMEM((4, *block), BF16),
             VMEM((4, *block), BF16),
@@ -617,40 +652,30 @@
             dma((steps,)), dma((steps,)), dma((steps, 2)), dma((steps, 4)), dma((steps,)), dma((steps, 2)),
             dma((steps,)), dma((steps,)), dma((n_z, 4)), dma((n_z, 4)),
         ],
-        compiler_params=pltpu.CompilerParams(collective_id=0, has_side_effects=True, vmem_limit_bytes=60 << 20),
+        compiler_params=pltpu.CompilerParams(collective_id=0, has_side_effects=True, vmem_limit_bytes=44 << 20),
         name="experts",
     )(send, w_gate, w_up, w_down)
 
 
-def settle_kernel(acc_ref, down_in, gate_in, step_in, log_in, proj_in, g_gate, g_up, g_down, d_gate, g_step, g_log, g_proj):
-    both = acc_ref[...].T
-    units = g_gate.shape[1]
-    g_gate[...] = both[:, 0:units]
-    g_up[...] = both[:, units : 2 * units]
-    for src, dst in ((down_in, g_down), (gate_in, d_gate), (step_in, g_step), (log_in, g_log), (proj_in, g_proj)):
-        dst[...] = src[...]
-
-
-def settle(acc_t, g_down, d_gate, g_step, g_log, g_proj):
-    parts = 4
-    units, model = g_down.shape
-
-    def rows(a):
-        return pl.BlockSpec((a.shape[0] // parts, a.shape[1]), lambda i: (i, 0))
-
-    def cols(a):
-        return pl.BlockSpec((a.shape[0], a.shape[1] // parts), lambda i: (0, i))
-
-    tall = jax.ShapeDtypeStruct((model, units), F32)
-    rest = [d_gate, g_step, g_log, g_proj]
+def settle_kernel(*refs):
+    n = len(refs) // 2
+    copies = [pltpu.make_async_copy(refs[k], refs[n + k], refs[2 * n].at[k]) for k in range(n)]
+    for copy in copies:
+        copy.start()
+    for copy in copies:
+        copy.wait()
+
+
+def settle(*values):
     return pl.pallas_call(
         settle_kernel,
-        grid=(parts,),
-        in_specs=[cols(acc_t), cols(g_down)] + [rows(a) for a in rest],
-        out_specs=[rows(tall), rows(tall), cols(g_down)] + [rows(a) for a in rest],
-        out_shape=[tall, tall] + [jax.ShapeDtypeStruct(a.shape, a.dtype) for a in [g_down] + rest],
+        in_specs=[pl.BlockSpec(memory_space=VMEM)] * len(values),
+        out_specs=[pl.BlockSpec(memory_space=pl.ANY)] * len(values),
+        out_shape=[jax.ShapeDtypeStruct(a.shape, a.dtype) for a in values],
+        scratch_shapes=[pltpu.SemaphoreType.DMA((len(values),))],
+        compiler_params=pltpu.CompilerParams(vmem_limit_bytes=16 << 20),
         name="settle",
-    )(acc_t, g_down, *rest)
+    )(*values)
 
 
 def on_device(resid, cotangent, routes, route_weight, w_gate, w_up, w_down, out_proj, gate_pre, log_decay,
@@ -659,9 +684,9 @@
     experts, n_tp = lax.axis_size("sp"), lax.axis_size("tp")
     cap = 2 * rows * routes.shape[1] // experts
     send, pick, cot_t = front(routes.T, route_weight.T, resid, cotangent, experts, cap, n_tp)
-    acc_t, grad_down, back = experts_pass(send, w_gate[0], w_up[0], w_down[0])
-    ended = tail(back, pick, cot_t, out_proj.T, gate_pre.T, log_decay.T, state_before.T, step_input.T)
-    grad_gate, grad_up, grad_down, d_gate, grad_step, grad_log, grad_proj = settle(acc_t, grad_down, *ended)
+    grads = experts_pass(send, w_gate[0], w_up[0], w_down[0])
+    ended = tail(grads[3], pick, cot_t, out_proj.T, gate_pre.T, log_decay.T, state_before.T, step_input.T)
+    grad_gate, grad_up, grad_down, d_gate, grad_step, grad_log, grad_proj = settle(*grads[:3], *ended)
     return grad_gate[None], grad_up[None], grad_down[None], grad_proj, d_gate.T, grad_step.T, grad_log.T
 
 

time: 182 us -> 157 us (0.86)
  Pallas kernels: 176 us -> 151 us
    pallas_call x2, Pallas kernels: 129 us -> 111 us  [the longest x1 108 us: experts_pass(): pl.pallas_call(experts_kernel, in_specs=[pl.BlockSpec(memory_space=pl.ANY...]
    pallas_call x1, Pallas kernels: 40.8 us -> 37.4 us  [tail(): pl.pallas_call(tail_kernel, in_specs=[pl.BlockSpec(memory_space=VMEM)] *...]
    pallas_call x1, Pallas kernels: 6.13 us -> 3.16 us  [front(): pl.pallas_call(functools.partial(front_kernel, experts, cap), grid_spec=p...]
    unnamed x22 -> x24, local copies, waits for them, and re-layouts: 4.14 us -> 4.23 us
where the time goes in v4:
time: 157 us; the launch traced here: 156 us
  Pallas kernels  151 us (96%)
  local copies, waits for them, and re-layouts  4.23 us (3%)
    pallas_call x1, Pallas kernels, experts_pass(): pl.pallas_call(experts_kernel, in_specs=[pl.BlockSpec(memory_space=pl.ANY...  108 us
    pallas_call x1, Pallas kernels, tail(): pl.pallas_call(tail_kernel, in_specs=[pl.BlockSpec(memory_space=VMEM)] *...  37.4 us
    unnamed x24, local copies, waits for them, and re-layouts  4.23 us
    pallas_call x1, Pallas kernels, front(): pl.pallas_call(functools.partial(front_kernel, experts, cap), grid_spec=p...  3.16 us

profile of v4, /device:TPU:16, one launch (start us, length us, event | category | flops | bytes accessed | tf_op | source)
XLA Modules:
  0.0 156.4 jit_solution(14083482847445334624)
XLA Ops:
  0.6 0.1 pad_add_fusion.tp_ref
  0.7 0.0 copy-start
  0.7 1.4 copy-done
  2.1 0.0 copy-start.1
  2.1 1.4 copy-done.1
  3.5 0.0 copy-start.10
  3.5 0.7 copy-done.10
  4.2 0.0 copy-start.11
  4.2 0.7 copy-done.11
  4.9 0.0 copy-start.5
  4.9 0.0 copy-start.6
  4.9 0.0 copy-start.7
  4.9 3.2 %front.1 = (bf16[2,32,96,256]{3,2,1,0:T(8,128)(2,1)S(1)}, bf16[1536,384]{1,0:T(8,128)(2,1)S(1)}, bf16[256,384]{1,0:T(8,128)(2,1)S(1)}) custom-call(s32[2]{0:T(128)S(1)} %pad_add_fusion.tp_ref, s32[2,384]{1,0:T(2,128)S(1)} %bitcast.26, f32[2,384]{1,0:T(2,128)S(1)} %bitcast.27, bf16[384,2048]{1,0:T(8,128)(2,1)S(1)} %copy-done, ...), custom_call_target="tpu_custom_call" | custom-call | tf_op jit(solution)/shard_map/front/pallas_call | solution.py:58
  8.1 0.0 copy-done.5
  8.1 0.0 copy-done.6
  8.1 0.0 copy-done.7
  8.1 0.0 copy-start.2
  8.1 0.0 copy-start.3
  8.1 0.0 copy-start.4
  8.1 0.0 copy-start.8
  8.2 0.0 copy-start.9
  8.2 108.5 %experts.1 = (f32[2048,128]{1,0:T(8,128)S(1)}, f32[2048,128]{1,0:T(8,128)S(1)}, f32[128,2048]{1,0:T(8,128)S(1)}, bf16[32,48,256]{2,1,0:T(8,128)(2,1)S(1)}) custom-call(bf16[2,32,96,256]{3,2,1,0:T(8,128)(2,1)S(1)} %get-tuple-element.25.send_ref, bf16[2048,128]{1,0:T(8,128)(2,1)S(1)} %bitcast.21, bf16[2048,128]{1,0:T(8,128)(2,1)S(1)} %bitcast.22, ...), custom_call_target="tpu_custom_call" | custom-call | tf_op jit(solution)/shard_map/experts/pallas_call | solution.py:628
  116.7 0.0 copy-done.2
  116.7 0.0 copy-done.3
  116.7 0.0 copy-done.4
  116.7 0.0 copy-done.8
  116.7 0.0 copy-done.9
  116.7 37.4 %tail.1 = (bf16[352,384]{1,0:T(8,128)(2,1)S(1)}, f32[352,384]{1,0:T(8,128)S(1)}, f32[352,384]{1,0:T(8,128)S(1)}, f32[64,352]{1,0:T(8,128)S(1)}) custom-call(bf16[32,48,256]{2,1,0:T(8,128)(2,1)S(1)} %get-tuple-element.29.back_ref, bf16[1536,384]{1,0:T(8,128)(2,1)S(1)} %get-tuple-element.30.pick_ref, bf16[256,384]{1,0:T(8,128)(2,1)S(1)} %get-tuple-element.31.cot_t_ref, ...), custom_call_target="tpu_custom_call" | custom-call | tf_op jit(solution)/shard_map/tail/pallas_call | solution.py:309
  154.1 2.2 %settle.1 = (f32[2048,128]{1,0:T(8,128)}, f32[2048,128]{1,0:T(8,128)}, f32[128,2048]{1,0:T(8,128)}, bf16[352,384]{1,0:T(8,128)(2,1)}, f32[352,384]{1,0:T(8,128)}, /*index=5*/f32[352,384]{1,0:T(8,128)}, f32[64,352]{1,0:T(8,128)}) custom-call(f32[2048,128]{1,0:T(8,128)S(1)} %get-tuple-element.26.refs_0_, f32[2048,128]{1,0:T(8,128)S(1)} %get-tuple-element.27.refs_1_, ...), custom_call_target="tpu_custom_call" | custom-call | tf_op jit(solution)/shard_map/settle/pallas_call | solution.py:670
Async XLA Ops:
  0.7 1.4 copy-start
  2.1 1.4 copy-start.1
  3.5 0.7 copy-start.10
  4.2 0.7 copy-start.11
  4.9 3.2 %copy-start.5 = (bf16[1,2048,128]{2,1,0:T(8,128)(2,1)S(1)}, bf16[1,2048,128]{2,1,0:T(8,128)(2,1)}, u32[]{:S(2)}) copy-start(bf16[1,2048,128]{2,1,0:T(8,128)(2,1)} %param.16) | copy-start | bytes 1572868
  4.9 3.2 %copy-start.6 = (bf16[1,2048,128]{2,1,0:T(8,128)(2,1)S(1)}, bf16[1,2048,128]{2,1,0:T(8,128)(2,1)}, u32[]{:S(2)}) copy-start(bf16[1,2048,128]{2,1,0:T(8,128)(2,1)} %param.17) | copy-start | bytes 1572868
  4.9 3.2 %copy-start.7 = (bf16[1,128,2048]{2,1,0:T(8,128)(2,1)S(1)}, bf16[1,128,2048]{2,1,0:T(8,128)(2,1)}, u32[]{:S(2)}) copy-start(bf16[1,128,2048]{2,1,0:T(8,128)(2,1)} %param.18) | copy-start | bytes 1572868
  8.1 108.6 %copy-start.2 = (bf16[2048,352]{0,1:T(8,128)(2,1)S(1)}, bf16[2048,352]{0,1:T(8,128)(2,1)}, u32[]{:S(2)}) copy-start(bf16[2048,352]{0,1:T(8,128)(2,1)} %param.19) | copy-start | bytes 4325380
  8.1 108.6 %copy-start.3 = (f32[384,352]{0,1:T(8,128)S(1)}, f32[384,352]{0,1:T(8,128)}, u32[]{:S(2)}) copy-start(f32[384,352]{0,1:T(8,128)} %param.21) | copy-start | bytes 1622020
  8.1 108.6 %copy-start.4 = (f32[384,352]{0,1:T(8,128)S(1)}, f32[384,352]{0,1:T(8,128)}, u32[]{:S(2)}) copy-start(f32[384,352]{0,1:T(8,128)} %param.22) | copy-start | bytes 1622020
  8.1 108.6 %copy-start.8 = (bf16[384,352]{0,1:T(8,128)(2,1)S(1)}, bf16[384,352]{0,1:T(8,128)(2,1)}, u32[]{:S(2)}) copy-start(bf16[384,352]{0,1:T(8,128)(2,1)} %param.20) | copy-start | bytes 811012
  8.2 108.6 %copy-start.9 = (bf16[384,352]{0,1:T(8,128)(2,1)S(1)}, bf16[384,352]{0,1:T(8,128)(2,1)}, u32[]{:S(2)}) copy-start(bf16[384,352]{0,1:T(8,128)(2,1)} %param.23) | copy-start | bytes 811012

commit v5 on v4

--- a/solution.py
+++ b/solution.py
@@ -112,13 +112,13 @@
     return lambda: pl.semaphore_wait(barrier, len(peers))
 
 
-def tail_kernel(back_ref, pick_ref, cot_t_ref, proj_ref, gate_ref, decay_ref, before_ref, step_ref,
+def tail_kernel(back_ref, pick_ref, cot_t_ref, proj_ref, decay_ref, before_ref, states, gelu, slope, mixed,
                 d_gate_ref, g_step_ref, g_log_ref, g_proj_ref,
-                rg, term, from_x, sums, from_z, ends, ends_x, row, ends_z, states, gelu, slope, mixed, dm, prod,
+                rg, term, from_x, sums, from_z, ends, ends_x, row, ends_z, dm, prod,
                 ag_send, ag_l, ag_r, ag_a, ag_d, x_send, x_recv, z_send, z_recv, e_send, ex_recv, ez_recv):
     sp, tp, z, x, right, left, across, flip = place()
     mate = tp + flip
-    channels, rows = gate_ref.shape
+    channels, rows = decay_ref.shape
     depth = rg.shape[1]
     half_rows = depth // 2
     part = channels // 2
@@ -147,28 +147,14 @@
     for copy in sent:
         copy.start()
 
-    def prepare(k):
-        at = pl.ds(k * part, part)
-        v = gate_ref[at, :].astype(F32)
-        decays = jnp.exp(decay_ref[at, :])
-        state = decays * before_ref[at, :] + step_ref[at, :].astype(F32)
-        th = jnp.tanh(ROOT * (v + 0.044715 * (v * v * v)))
-        act = 0.5 * v * (1.0 + th)
-        gelu[at, :] = act
-        states[at, :] = state
-        slope[at, :] = 0.5 * (1.0 + th) + 0.5 * v * (1.0 - th * th) * (ROOT * (1.0 + 3.0 * 0.044715 * (v * v)))
-        mixed[at, :] = (act * state).astype(BF16)
-
     def pass_on(ref, k, arrived, recv, to):
         moved(ref, k, arrived, to).wait_recv()
         copy = moved(ref, k, recv, to)
         copy.start()
         sent.append(copy)
 
-    prepare(0)
     pass_on(half(left, 0), 5, ag_l.at[0], ag_a.at[0], right)
     pass_on(half(right, 1), 6, ag_r.at[1], ag_a.at[1], left)
-    prepare(1)
 
     crossing = []
 
@@ -299,8 +285,8 @@
         copy.wait_send()
 
 
-def tail(back, pick, cot_t, proj, gate, decay, before, step):
-    channels, rows = gate.shape
+def tail(back, pick, cot_t, proj, decay, before, states, gelu, slope, mixed):
+    channels, rows = decay.shape
     depth = cot_t.shape[0]
     flat = (channels, rows)
     lines = 8 * depth // 32
@@ -308,7 +294,7 @@
     dma = pltpu.SemaphoreType.DMA
     return pl.pallas_call(
         tail_kernel,
-        in_specs=[pl.BlockSpec(memory_space=VMEM)] * 8,
+        in_specs=[pl.BlockSpec(memory_space=VMEM)] * 10,
         out_specs=[pl.BlockSpec(memory_space=VMEM)] * 4,
         out_shape=[jax.ShapeDtypeStruct(s, d) for s, d in outs],
         scratch_shapes=[
@@ -323,26 +309,23 @@
             VMEM((8, 8, channels), F32),
             VMEM(flat, F32),
             VMEM(flat, F32),
-            VMEM(flat, F32),
-            VMEM(flat, BF16),
-            VMEM(flat, F32),
-            VMEM(flat, F32),
             dma((11,)), dma((2,)), dma((2,)), dma((2,)), dma((5,)),
             dma((8, 3)), dma((8, 3)), dma((8,)), dma((8,)), dma((10,)), dma((3,)), dma((7,)),
         ],
         compiler_params=pltpu.CompilerParams(collective_id=1, has_side_effects=True, vmem_limit_bytes=24 << 20),
         name="tail",
-    )(back, pick, cot_t, proj, gate, decay, before, step)
+    )(back, pick, cot_t, proj, decay, before, states, gelu, slope, mixed)
 
 
 N_SENDS = 14
-ORDER = (0, 1, 3, 5, 4, 2, 6, 7)
-FAR = (2, 5)
-
-
-def experts_kernel(send_ref, w_gate_ref, w_up_ref, w_down_ref,
-                   g_gate_ref, g_up_ref, g_down_ref, back_ref,
-                   buf, w_cat, w_cat_t, w_down, w_down_t, acc_t, acc_down, g_tall, loads, stores, parts, from_mate, pair, from_far, from_left, from_right, ret, back,
+ORDER = (0, 1, 7, 3, 5, 4, 2, 6)
+FAR = (3, 6)
+
+
+def experts_kernel(send_ref, w_gate_ref, w_up_ref, w_down_ref, gate_in, decay_in, before_in, step_in,
+                   g_gate_ref, g_up_ref, g_down_ref, back_ref, states, gelu, slope, mixed,
+                   gate_ref, decay_ref, before_ref, step_ref,
+                   buf, w_cat, w_cat_t, w_down, w_down_t, acc_t, loads, parts, from_mate, pair, from_far, from_left, from_right, ret, back,
                    a_send, a_recv, far_send, far_recv, sends, yl, yr, ya, ym, pm, fa, fl, fr, b_send, b_recv):
     sp, tp, z, x, right, left, across, flip = place()
     mate = tp + flip
@@ -386,6 +369,10 @@
         pltpu.make_async_copy(w_gate_ref, w_cat.at[:, 0:128], loads.at[0]),
         pltpu.make_async_copy(w_up_ref, w_cat.at[:, 128:256], loads.at[1]),
         pltpu.make_async_copy(w_down_ref, w_down, loads.at[2]),
+        pltpu.make_async_copy(gate_in, gate_ref, loads.at[3]),
+        pltpu.make_async_copy(decay_in, decay_ref, loads.at[4]),
+        pltpu.make_async_copy(before_in, before_ref, loads.at[5]),
+        pltpu.make_async_copy(step_in, step_ref, loads.at[6]),
     ]
     arrive()
     pltpu.make_async_copy(send_ref.at[0, sp], buf.at[tp, sp], a_recv.at[0, x]).start()
@@ -416,12 +403,24 @@
             for copy in weights:
                 copy.wait()
             acc_t[...] = jnp.zeros_like(acc_t)
-            acc_down[...] = jnp.zeros_like(acc_down)
+            g_down_ref[...] = jnp.zeros_like(g_down_ref)
 
         for k in range(2):
             at = pl.ds(pl.multiple_of((2 * t + k) * depth, depth), depth)
             w_cat_t[:, at] = w_cat[at, :].astype(F32).T.astype(BF16)
             w_down_t[at, :] = w_down[:, at].astype(F32).T.astype(BF16)
+
+    def activate(k):
+        part = gate_ref.shape[0] // 2
+        at = pl.ds(k * part, part)
+        v = gate_ref[at, :].astype(F32)
+        state = jnp.exp(decay_ref[at, :]) * before_ref[at, :] + step_ref[at, :].astype(F32)
+        th = jnp.tanh(ROOT * (v + 0.044715 * (v * v * v)))
+        act = 0.5 * v * (1.0 + th)
+        gelu[at, :] = act
+        states[at, :] = state
+        slope[at, :] = 0.5 * (1.0 + th) + 0.5 * v * (1.0 - th * th) * (ROOT * (1.0 + 3.0 * 0.044715 * (v * v)))
+        mixed[at, :] = (act * state).astype(BF16)
 
     def first(s):
         return source(lax.div(s, 2)) + 2 * lax.rem(s, 2)
@@ -523,7 +522,7 @@
         for j in range(8):
             cols = slice(j * depth, (j + 1) * depth)
             acc_t[:, cols] += contract(d_both_t, rows_of(j), 1, 0)
-            acc_down[:, cols] += contract(hidden_t, cots_of(j), 1, 0)
+            g_down_ref[:, cols] += contract(hidden_t, cots_of(j), 1, 0)
 
     def pair_up(s):
         blk = pl.ds(first(s), 2)
@@ -568,18 +567,16 @@
         def _():
             prepare(t)
 
+        for k in range(2):
+            @pl.when(t == 3 + k)
+            def _():
+                activate(k)
+
     for j in range(8):
         cols = slice(j * depth, (j + 1) * depth)
         both = acc_t[:, cols].T
-        g_tall[0, cols, :] = both[:, 0:128]
-        g_tall[1, cols, :] = both[:, 128:256]
-    results = [
-        pltpu.make_async_copy(g_tall.at[0], g_gate_ref, stores.at[0]),
-        pltpu.make_async_copy(g_tall.at[1], g_up_ref, stores.at[1]),
-        pltpu.make_async_copy(acc_down, g_down_ref, stores.at[2]),
-    ]
-    for copy in results:
-        copy.start()
+        g_gate_ref[cols, :] = both[:, 0:128]
+        g_up_ref[cols, :] = both[:, 128:256]
 
     @pl.loop(0, n_z)
     def _(i):
@@ -587,8 +584,6 @@
             wait(back.at[target(i) + q], b_recv.at[i, q])
 
     back_ref[...] = back[...]
-    for copy in results:
-        copy.wait()
 
     @pl.loop(0, steps)
     def _(s):
@@ -616,7 +611,7 @@
                 back_copy(i, d).wait_send()
 
 
-def experts_pass(send, w_gate, w_up, w_down):
+def experts_pass(send, w_gate, w_up, w_down, gate, decay, before, step):
     _, n_sp, both_caps, depth = send.shape
     model, units = w_gate.shape
     cap = both_caps // 2
@@ -625,21 +620,25 @@
     steps = 2 * n_z
     dma = pltpu.SemaphoreType.DMA
     outs = [((model, units), F32), ((model, units), F32), ((units, model), F32), (block, BF16)]
+    flat = gate.shape
+    outs += [(flat, F32), (flat, F32), (flat, F32), (flat, BF16)]
     return pl.pallas_call(
         experts_kernel,
-        in_specs=[pl.BlockSpec(memory_space=pl.ANY)] * 4,
-        out_specs=[pl.BlockSpec(memory_space=pl.ANY)] * 3 + [pl.BlockSpec(memory_space=VMEM)],
+        in_specs=[pl.BlockSpec(memory_space=pl.ANY)] * 8,
+        out_specs=[pl.BlockSpec(memory_space=VMEM)] * 8,
         out_shape=[jax.ShapeDtypeStruct(s, d) for s, d in outs],
         scratch_shapes=[
+            VMEM(flat, BF16),
+            VMEM(flat, F32),
+            VMEM(flat, F32),
+            VMEM(flat, BF16),
             VMEM((8, n_sp, both_caps, depth), BF16),
             VMEM((model, 2 * units), BF16),
             VMEM((2 * units, model), BF16),
             VMEM((units, model), BF16),
             VMEM((model, units), BF16),
             VMEM((2 * units, model), F32),
-            VMEM((units, model), F32),
-            VMEM((2, model, units), F32),
-            dma((3,)), dma((3,)),
+            dma((7,)),
             VMEM((2, 4, *block), BF16),
             VMEM((4, *block), BF16),
             VMEM((4, *block), BF16),
@@ -652,9 +651,9 @@
             dma((steps,)), dma((steps,)), dma((steps, 2)), dma((steps, 4)), dma((steps,)), dma((steps, 2)),
             dma((steps,)), dma((steps,)), dma((n_z, 4)), dma((n_z, 4)),
         ],
-        compiler_params=pltpu.CompilerParams(collective_id=0, has_side_effects=True, vmem_limit_bytes=44 << 20),
+        compiler_params=pltpu.CompilerParams(collective_id=0, has_side_effects=True, vmem_limit_bytes=38 << 20),
         name="experts",
-    )(send, w_gate, w_up, w_down)
+    )(send, w_gate, w_up, w_down, gate, decay, before, step)
 
 
 def settle_kernel(*refs):
@@ -684,9 +683,10 @@
     experts, n_tp = lax.axis_size("sp"), lax.axis_size("tp")
     cap = 2 * rows * routes.shape[1] // experts
     send, pick, cot_t = front(routes.T, route_weight.T, resid, cotangent, experts, cap, n_tp)
-    grads = experts_pass(send, w_gate[0], w_up[0], w_down[0])
-    ended = tail(grads[3], pick, cot_t, out_proj.T, gate_pre.T, log_decay.T, state_before.T, step_input.T)
-    grad_gate, grad_up, grad_down, d_gate, grad_step, grad_log, grad_proj = settle(*grads[:3], *ended)
+    decay, before = log_decay.T, state_before.T
+    done = experts_pass(send, w_gate[0], w_up[0], w_down[0], gate_pre.T, decay, before, step_input.T)
+    ended = tail(done[3], pick, cot_t, out_proj.T, decay, before, *done[4:])
+    grad_gate, grad_up, grad_down, d_gate, grad_step, grad_log, grad_proj = settle(*done[:3], *ended)
     return grad_gate[None], grad_up[None], grad_down[None], grad_proj, d_gate.T, grad_step.T, grad_log.T
 
 

time: 157 us -> 157 us (level)
    pallas_call x1, Pallas kernels: 37.4 us -> 38.9 us  [tail(): pl.pallas_call(tail_kernel, in_specs=[pl.BlockSpec(memory_space=VMEM)] *...]
where the time goes in v5:
time: 157 us
  Pallas kernels  151 us (96%)
  local copies, waits for them, and re-layouts  4.22 us (3%)
    pallas_call x1, Pallas kernels, experts_pass(): pl.pallas_call(experts_kernel, in_specs=[pl.BlockSpec(memory_space=pl.ANY...  107 us
    pallas_call x1, Pallas kernels, tail(): pl.pallas_call(tail_kernel, in_specs=[pl.BlockSpec(memory_space=VMEM)] *...  38.9 us
    unnamed x24, local copies, waits for them, and re-layouts  4.22 us
    pallas_call x1, Pallas kernels, front(): pl.pallas_call(functools.partial(front_kernel, experts, cap), grid_spec=p...  3.17 us

profile of v5, /device:TPU:16, one launch (start us, length us, event | category | flops | bytes accessed | tf_op | source)
XLA Modules:
  0.0 156.5 jit_solution(10321146686715008328)
XLA Ops:
  0.6 0.1 pad_add_fusion.tp_ref
  0.7 0.0 copy-start
  0.7 1.4 copy-done
  2.1 0.0 copy-start.1
  2.1 1.4 copy-done.1
  3.5 0.0 copy-start.10
  3.5 0.7 copy-done.10
  4.2 0.0 copy-start.11
  4.2 0.7 copy-done.11
  4.9 0.0 copy-start.2
  4.9 0.0 copy-start.3
  4.9 0.0 copy-start.5
  4.9 0.0 copy-start.6
  4.9 0.0 copy-start.7
  4.9 0.0 copy-start.8
  4.9 0.0 copy-start.9
  4.9 3.2 %front.1 = (bf16[2,32,96,256]{3,2,1,0:T(8,128)(2,1)S(1)}, bf16[1536,384]{1,0:T(8,128)(2,1)S(1)}, bf16[256,384]{1,0:T(8,128)(2,1)S(1)}) custom-call(s32[2]{0:T(128)S(1)} %pad_add_fusion.tp_ref, s32[2,384]{1,0:T(2,128)S(1)} %bitcast.28, f32[2,384]{1,0:T(2,128)S(1)} %bitcast.29, bf16[384,2048]{1,0:T(8,128)(2,1)S(1)} %copy-done, ...), custom_call_target="tpu_custom_call" | custom-call | tf_op jit(solution)/shard_map/front/pallas_call | solution.py:58
  8.1 0.0 copy-done.2
  8.1 0.0 copy-done.3
  8.1 0.0 copy-done.5
  8.1 0.0 copy-done.6
  8.2 0.0 copy-done.7
  8.2 0.0 copy-done.8
  8.2 0.0 copy-done.9
  8.2 0.0 copy-start.4
  8.2 107.0 %experts.1 = (f32[2048,128]{1,0:T(8,128)S(1)}, f32[2048,128]{1,0:T(8,128)S(1)}, f32[128,2048]{1,0:T(8,128)S(1)}, bf16[32,48,256]{2,1,0:T(8,128)(2,1)S(1)}, f32[3...) custom-call(bf16[2,32,96,256]{3,2,1,0:T(8,128)(2,1)S(1)} %get-tuple-element.2, ...), custom_call_target="tpu_custom_call" | custom-call | tf_op jit(solution)/shard_map/experts/pallas_call | solution.py:625
  115.2 0.0 copy-done.4
  115.2 38.9 %tail.1 = (bf16[352,384]{1,0:T(8,128)(2,1)S(1)}, f32[352,384]{1,0:T(8,128)S(1)}, f32[352,384]{1,0:T(8,128)S(1)}, f32[64,352]{1,0:T(8,128)S(1)}) custom-call(bf16[32,48,256]{2,1,0:T(8,128)(2,1)S(1)} %get-tuple-element.33.back_ref, bf16[1536,384]{1,0:T(8,128)(2,1)S(1)} %get-tuple-element.34.pick_ref, bf16[256,384]{1,0:T(8,128)(2,1)S(1)} %get-tuple-element.35.cot_t_ref, ...), custom_call_target="tpu_custom_call" | custom-call | tf_op jit(solution)/shard_map/tail/pallas_call | solution.py:295
  154.2 2.2 %settle.1 = (f32[2048,128]{1,0:T(8,128)}, f32[2048,128]{1,0:T(8,128)}, f32[128,2048]{1,0:T(8,128)}, bf16[352,384]{1,0:T(8,128)(2,1)}, f32[352,384]{1,0:T(8,128)}, /*index=5*/f32[352,384]{1,0:T(8,128)}, f32[64,352]{1,0:T(8,128)}) custom-call(f32[2048,128]{1,0:T(8,128)S(1)} %get-tuple-element.30.refs_0_, f32[2048,128]{1,0:T(8,128)S(1)} %get-tuple-element.31.refs_1_, ...), custom_call_target="tpu_custom_call" | custom-call | tf_op jit(solution)/shard_map/settle/pallas_call | solution.py:669
Async XLA Ops:
  0.7 1.4 copy-start
  2.1 1.4 copy-start.1
  3.5 0.7 copy-start.10
  4.2 0.7 copy-start.11
  4.9 3.2 %copy-start.2 = (f32[384,352]{0,1:T(8,128)S(1)}, f32[384,352]{0,1:T(8,128)}, u32[]{:S(2)}) copy-start(f32[384,352]{0,1:T(8,128)} %param.21) | copy-start | bytes 1622020
  4.9 3.2 %copy-start.3 = (f32[384,352]{0,1:T(8,128)S(1)}, f32[384,352]{0,1:T(8,128)}, u32[]{:S(2)}) copy-start(f32[384,352]{0,1:T(8,128)} %param.22) | copy-start | bytes 1622020
  4.9 3.2 %copy-start.5 = (bf16[1,2048,128]{2,1,0:T(8,128)(2,1)S(1)}, bf16[1,2048,128]{2,1,0:T(8,128)(2,1)}, u32[]{:S(2)}) copy-start(bf16[1,2048,128]{2,1,0:T(8,128)(2,1)} %param.16) | copy-start | bytes 1572868
  4.9 3.2 %copy-start.6 = (bf16[1,2048,128]{2,1,0:T(8,128)(2,1)S(1)}, bf16[1,2048,128]{2,1,0:T(8,128)(2,1)}, u32[]{:S(2)}) copy-start(bf16[1,2048,128]{2,1,0:T(8,128)(2,1)} %param.17) | copy-start | bytes 1572868
  4.9 3.3 %copy-start.7 = (bf16[1,128,2048]{2,1,0:T(8,128)(2,1)S(1)}, bf16[1,128,2048]{2,1,0:T(8,128)(2,1)}, u32[]{:S(2)}) copy-start(bf16[1,128,2048]{2,1,0:T(8,128)(2,1)} %param.18) | copy-start | bytes 1572868
  4.9 3.2 %copy-start.8 = (bf16[384,352]{0,1:T(8,128)(2,1)S(1)}, bf16[384,352]{0,1:T(8,128)(2,1)}, u32[]{:S(2)}) copy-start(bf16[384,352]{0,1:T(8,128)(2,1)} %param.20) | copy-start | bytes 811012
  4.9 3.2 %copy-start.9 = (bf16[384,352]{0,1:T(8,128)(2,1)S(1)}, bf16[384,352]{0,1:T(8,128)(2,1)}, u32[]{:S(2)}) copy-start(bf16[384,352]{0,1:T(8,128)(2,1)} %param.23) | copy-start | bytes 811012
  8.2 107.0 %copy-start.4 = (bf16[2048,352]{0,1:T(8,128)(2,1)S(1)}, bf16[2048,352]{0,1:T(8,128)(2,1)}, u32[]{:S(2)}) copy-start(bf16[2048,352]{0,1:T(8,128)(2,1)} %param.19) | copy-start | bytes 4325380
